TPU v7x, 256 devices: a 8x8x2 block of a 8x8x16 slice. The times are simulated.
256 devices in a mesh: grp: 2 (over z), ep: 64 (over y, x), tp: 2 (over core).
Axes of the slice: x: 8, y: 8, z: 2, core: 2. Of those that a mesh axis runs over, the one named last changes fastest.
The devices are a block of a 8x8x16 slice.
Arguments:
- layer_input: bfloat16 [4096, 2048], P(('grp', 'ep')), parts along dimension 0, may hold values from -6 to 6
- ssm_state: float32 [2, 4096, 32, 64], P(None, ('grp', 'ep'), 'tp'), parts along dimension 1, may hold values from -4 to 4
- w_input: bfloat16 [2048, 512], P(None, 'tp'), may hold values from -0.125 to 0.125
- decay_rate: float32 [32, 64], P('tp'), may hold values from 0.05 to 2
- frequency: float32 [32, 64], P('tp'), may hold values from 0 to 20
- step_log: float32 [32], P('tp'), may hold values from -2.3 to 0
- input_map: float32 [2, 32, 64, 16], P(None, 'tp'), may hold values from -1 to 1
- output_map: float32 [2, 32, 16, 64], P(None, 'tp'), may hold values from -0.75 to 0.75
- skip_gain: float32 [32, 16], P('tp'), may hold values from -3 to 3
- glu_weight: bfloat16 [512, 512], replicated, may hold values from -0.25 to 0.25
- mix_out: bfloat16 [512, 2048], replicated, may hold values from -0.75 to 0.75
- norm_gain: float32 [2048], replicated, may hold values from 0.1 to 6, as said below
- norm_shift: float32 [2048], replicated, may hold values from -2 to 2
- route_ids: int32 [4096, 6], P(('grp', 'ep')), parts along dimension 0, may hold values from 0 to 63, all different within a row; in each aligned block of 32 rows (0 to 31, 32 to 63, ...) at most 6 rows name the same one
- route_weights: float32 [4096, 6], P(('grp', 'ep')), parts along dimension 0, may hold values from 0.1 to 1
- gate_expert: bfloat16 [64, 2048, 512], P('ep', None, 'tp'), may hold values from -0.125 to 0.125
- up_expert: bfloat16 [64, 2048, 512], P('ep', None, 'tp'), may hold values from -0.125 to 0.125
- down_expert: bfloat16 [64, 512, 2048], P('ep', 'tp'), may hold values from -0.25 to 0.25
- gate_shared: bfloat16 [2048, 512], P(None, 'tp'), may hold values from -0.125 to 0.125
- up_shared: bfloat16 [2048, 512], P(None, 'tp'), may hold values from -0.125 to 0.125
- down_shared: bfloat16 [512, 2048], P('tp'), may hold values from -0.25 to 0.25
- dense_in: bfloat16 [1024, 2048], P('ep'), may hold values from -0.125 to 0.125
- dense_out: bfloat16 [1024, 2048], P('ep', 'tp'), may hold values from -0.1875 to 0.1875
- branch_gate: bfloat16 [2048], replicated, may hold values from -0.125 to 0.125
- final_gain: float32 [2048], P('tp'), may hold values from 0.1 to 1.9
- final_shift: float32 [2048], P('tp'), may hold values from -2 to 2
Outputs:
- layer_output: bfloat16 [4096, 2048], P(('grp', 'ep'), 'tp'), parts along dimension 0
- new_state: float32 [2, 4096, 32, 64], P(None, ('grp', 'ep'), 'tp'), parts along dimension 1
There are 2 independent parts, one for each index of `grp`. A program takes and returns all parts, laid end to end along the dimension named above; an argument that names none is the same for every part. Nothing has to cross between parts.
Inputs may be any that keep to these rules, and one draw needn't show every extreme that they name: `route_ids`: each row names 6 different experts; within each aligned block of 32 rows no expert is named more than 6 times, and in some block one expert is named exactly 6 times. `norm_gain`: positive gains.
All inputs are finite; a program needn't handle non-finite values.
Results may differ from a plain program's by a relative error of at most 0.015.
Values may be sent and summed in bfloat16 or wider, within the bound.
A program may use at most 128 MiB of HBM per device.

v0:
```python
import jax
import jax.numpy as jnp
from jax import lax
from jax.sharding import PartitionSpec as P

residual_alpha = 1.681792830507429
route_scale = 2.5
norm_eps = 1e-05
highest = lax.Precision.HIGHEST


def cut_along(shard, dim, peers):
    shape = shard.shape
    tiles = shard.reshape(*shape[:dim], peers, shape[dim] // peers, *shape[dim + 1 :])
    return jnp.moveaxis(tiles, dim, 0)


def sum_at_owner(shard, axis, dim):
    peers = lax.axis_size(axis)
    tiles = lax.all_to_all(cut_along(shard, dim, peers), axis, 0, 0, tiled=True)
    return jnp.sum(tiles.astype(jnp.float32), axis=0)


def from_everyone(shard, axis):
    peers = lax.axis_size(axis)
    return lax.all_to_all(
        jnp.broadcast_to(shard[None], (peers, *shard.shape)), axis, 0, 0, tiled=True
    )


def in_order(tiles, dim):
    shape = list(tiles.shape[1:])
    shape[dim] *= tiles.shape[0]
    return jnp.moveaxis(tiles, 0, dim).reshape(shape)


def gathered_copies(shard, axis, dim):
    tiles = from_everyone(shard, axis)
    return in_order(tiles, dim)


def in_one_piece(arrays, axis, dim, along):
    widths = [a.shape[along] for a in arrays]
    both = jnp.concatenate(arrays, axis=along)
    out = lax.all_gather(both, axis, axis=dim, tiled=True)
    return tuple(jnp.split(out, [sum(widths[:k]) for k in range(1, len(widths))], axis=along))


def gathered_total(shard, axis):
    return lax.all_gather(shard, axis).sum(0)


def state_update(
    inputs, ssm_state, decay_rate, frequency, step_log, input_map, output_map, skip_gain
):
    step_size = jnp.exp(step_log)[:, None]
    magnitude = jnp.exp(-decay_rate * step_size)
    rotation = frequency * step_size
    decay_re = magnitude * jnp.cos(rotation)
    decay_im = magnitude * jnp.sin(rotation)
    eigen_re = -decay_rate
    denominator = eigen_re * eigen_re + frequency * frequency
    factor_re = ((decay_re - 1.0) * eigen_re + decay_im * frequency) / denominator
    factor_im = (decay_im * eigen_re - (decay_re - 1.0) * frequency) / denominator
    drive_re = factor_re[..., None] * input_map[0] - factor_im[..., None] * input_map[1]
    drive_im = factor_re[..., None] * input_map[1] + factor_im[..., None] * input_map[0]
    pushed_re = jnp.einsum("gpm,tgm->tgp", drive_re, inputs, precision=highest)
    pushed_im = jnp.einsum("gpm,tgm->tgp", drive_im, inputs, precision=highest)
    new_re = decay_re * ssm_state[0] - decay_im * ssm_state[1] + pushed_re
    new_im = decay_re * ssm_state[1] + decay_im * ssm_state[0] + pushed_im
    response = (
        jnp.einsum("gmp,tgp->tgm", output_map[0], new_re, precision=highest)
        - jnp.einsum("gmp,tgp->tgm", output_map[1], new_im, precision=highest)
        + skip_gain * inputs
    )
    return (response, jnp.stack([new_re, new_im]))


def layer_norm_rows(values, gain, shift):
    mean = jnp.mean(values, axis=1, keepdims=True)
    variance = jnp.mean(jnp.square(values - mean), axis=1, keepdims=True)
    return (values - mean) * lax.rsqrt(variance + norm_eps) * gain + shift


def expert_terms(slot_rows, gate_weight, up_weight, down_weight):
    gate_part = jnp.einsum(
        "send,edf->senf", slot_rows, gate_weight, preferred_element_type=jnp.float32
    )
    up_part = jnp.einsum("send,edf->senf", slot_rows, up_weight, preferred_element_type=jnp.float32)
    hidden = (jax.nn.silu(gate_part) * up_part).astype(jnp.bfloat16)
    return jnp.einsum("senf,efd->send", hidden, down_weight, preferred_element_type=jnp.float32)


def finish_experts(partial_value):
    summed = sum_at_owner(partial_value.astype(jnp.bfloat16), "tp", 3).astype(jnp.bfloat16)
    return lax.all_to_all(summed, "ep", split_axis=0, concat_axis=0, tiled=True)


def dense_rows(rows, in_piece, out_piece):
    hidden = jax.nn.gelu(
        lax.dot_general(
            rows, in_piece, (((1,), (1,)), ((), ())), preferred_element_type=jnp.float32
        )
    ).astype(jnp.bfloat16)
    return jnp.dot(hidden, out_piece, preferred_element_type=jnp.float32)


def body(
    layer_input,
    ssm_state,
    w_input,
    decay_rate,
    frequency,
    step_log,
    input_map,
    output_map,
    skip_gain,
    glu_weight,
    mix_out,
    norm_gain,
    norm_shift,
    route_ids,
    route_weights,
    gate_expert,
    up_expert,
    down_expert,
    gate_shared,
    up_shared,
    down_shared,
    dense_in,
    dense_out,
    branch_gate,
    final_gain,
    final_shift,
):
    count_ep = lax.axis_size("ep")
    count_tp = lax.axis_size("tp")
    core = lax.axis_index("tp")
    seq_rows, width = layer_input.shape
    local_groups, channels = skip_gain.shape
    projected = jnp.dot(layer_input, w_input, preferred_element_type=jnp.float32).astype(
        jnp.bfloat16
    )
    inputs = projected.astype(jnp.float32).reshape(seq_rows, local_groups, channels)
    response, new_state = state_update(
        inputs, ssm_state, decay_rate, frequency, step_log, input_map, output_map, skip_gain
    )
    activated = jax.nn.gelu(response.reshape(seq_rows, local_groups * channels)).astype(
        jnp.bfloat16
    )
    every_channel = gathered_copies(activated, "tp", 1)
    glu_out = (
        every_channel.astype(jnp.float32)
        * jax.nn.sigmoid(jnp.dot(every_channel, glu_weight, preferred_element_type=jnp.float32))
    ).astype(jnp.bfloat16)
    mixed = jnp.dot(glu_out, mix_out, preferred_element_type=jnp.float32).astype(jnp.bfloat16)
    normed = layer_norm_rows(
        residual_alpha * layer_input.astype(jnp.float32) + mixed.astype(jnp.float32),
        norm_gain,
        norm_shift,
    ).astype(jnp.bfloat16)
    top_k = route_ids.shape[1]
    local_experts = gate_expert.shape[0]
    experts = local_experts * count_ep
    capacity = count_tp * max(1, min(seq_rows // count_tp, seq_rows * top_k // experts))
    flat_ids = route_ids.reshape(-1)
    hits = (flat_ids[:, None] == jnp.arange(experts, dtype=jnp.int32)[None, :]).astype(jnp.int32)
    ranks = jnp.sum((jnp.cumsum(hits, axis=0) - hits) * hits, axis=1)
    target = flat_ids * capacity + ranks
    outgoing = (
        jnp.zeros((experts * capacity, width), jnp.bfloat16)
        .at[target]
        .set(jnp.repeat(normed, top_k, axis=0))
        .reshape(count_ep, local_experts, capacity, width)
    )
    portion = capacity // count_tp
    own_slots = lax.dynamic_slice_in_dim(outgoing, core * portion, portion, 2)
    arrived = lax.all_to_all(own_slots, "ep", split_axis=0, concat_axis=0, tiled=True)
    slot_rows = gathered_copies(arrived, "tp", 2)
    returned = finish_experts(expert_terms(slot_rows, gate_expert, up_expert, down_expert))
    half_width = returned.shape[3]
    picked = returned.reshape(experts * capacity, half_width)[target].astype(jnp.float32)
    weights = route_weights / jnp.sum(route_weights, axis=1, keepdims=True) * route_scale
    routed = jnp.sum(picked.reshape(seq_rows, top_k, half_width) * weights[:, :, None], axis=1)
    shared_gate = jnp.dot(normed, gate_shared, preferred_element_type=jnp.float32)
    shared_up = jnp.dot(normed, up_shared, preferred_element_type=jnp.float32)
    shared_hidden = (jax.nn.silu(shared_gate) * shared_up).astype(jnp.bfloat16)
    shared_part = jnp.dot(shared_hidden, down_shared, preferred_element_type=jnp.float32)
    shared = sum_at_owner(shared_part.astype(jnp.bfloat16), "tp", 1).astype(jnp.bfloat16)
    pieces = in_one_piece((dense_in, dense_out), "ep", 0, 1)
    dense = dense_rows(normed, pieces[0], pieces[1])
    own_normed = lax.dynamic_slice_in_dim(normed, core * half_width, half_width, 1).astype(
        jnp.float32
    )
    branch = jax.nn.sigmoid(jnp.dot(normed, branch_gate, preferred_element_type=jnp.float32))
    total = (
        residual_alpha * own_normed + routed + shared.astype(jnp.float32) + branch[:, None] * dense
    )
    row_sum, row_squares = (
        gathered_total(jnp.sum(total, axis=1), "tp"),
        gathered_total(jnp.sum(total * total, axis=1), "tp"),
    )
    mean = row_sum / width
    variance = row_squares / width - mean * mean
    layer_output = (
        (total - mean[:, None]) * lax.rsqrt(variance[:, None] + norm_eps) * final_gain + final_shift
    ).astype(jnp.bfloat16)
    return (layer_output, new_state)


def solution(mesh):
    placed = (
        P(("grp", "ep"), None),
        P(None, ("grp", "ep"), "tp", None),
        P(None, "tp"),
        P("tp", None),
        P("tp", None),
        P("tp"),
        P(None, "tp", None, None),
        P(None, "tp", None, None),
        P("tp", None),
        P(),
        P(),
        P(),
        P(),
        P(("grp", "ep"), None),
        P(("grp", "ep"), None),
        P("ep", None, "tp"),
        P("ep", None, "tp"),
        P("ep", "tp", None),
        P(None, "tp"),
        P(None, "tp"),
        P("tp", None),
        P("ep", None),
        P("ep", "tp"),
        P(),
        P("tp"),
        P("tp"),
    )
    return jax.shard_map(
        body,
        mesh=mesh,
        in_specs=placed,
        out_specs=(P(("grp", "ep"), "tp"), P(None, ("grp", "ep"), "tp", None)),
        check_vma=False,
    )
```

profile of v0, /device:TPU:513, one launch (start us, length us, event | category | flops | bytes accessed | tf_op | source)
XLA Modules:
  0.0 177.3 jit_solution(3020654767425148184)
XLA Ops:
  7.2 0.1 all-gather.4.cloned.1.call-start
  7.3 1.6 pad_maximum_fusion.1
  9.0 0.7 exp.20
  9.7 1.6 convolution_convert_fusion.3
  11.3 0.1 copy.57
  11.4 0.1 add_divide_fusion
  11.6 0.4 fusion.9
  12.1 1.5 fusion.57
  13.6 0.4 fusion.8
  14.0 0.7 copy-done.2
  14.7 0.5 fusion.12
  15.3 0.1 copy.62
  15.4 0.6 broadcast_in_dim.10
  16.0 23.7 %all-to-all-start = ((bf16[2,32,256]{2,1,0:T(8,128)(2,1)}), bf16[2,32,256]{2,1,0:T(8,128)(2,1)S(1)}, u32[]{:S(2)}, u32[]{:S(2)}) async-start(bf16[2,32,256]{2,1,0:T(8,128)(2,1)} %broadcast_in_dim.10), calls=%async_computation | async-start | bytes 65536 | tf_op jit(solution)/shard_map/all_to_all | solution.py:26
  39.7 1.0 all-to-all-done
  40.8 0.8 fusion.104
  41.5 0.2 multiply_reduce_fusion.1
  41.8 0.1 add_convert_fusion
  41.9 0.1 broadcast_in_dim.12
  42.1 1.2 reshape.195
  43.2 0.1 copy.65
  43.3 0.1 eq.22
  43.4 0.6 reduce-window.6
  44.1 0.2 slice_reduce_fusion
  44.3 0.1 copy.64
  44.4 0.1 mul.322
  44.5 0.1 bitcast_bitcast_fusion.2
  44.6 3.8 %scatter_custom_fusion = bf16[384,2048]{1,0:T(8,128)(2,1)} fusion(s32[192]{0:T(256)S(1)} %bitcast.179, bf16[192,2048]{1,0:T(8,128)(2,1)} %reshape.195, bf16[]{:T(256)} %constant.15.clone.1), kind=kCustom, calls=%fused_computation.45 | custom fusion | bytes 1573376 | tf_op jit(solution)/shard_map/scatter | solution.py:173
  48.4 3.7 %reshape.172 = bf16[64,1,6,2048]{3,2,0,1:T(8,128)(2,1)} reshape(bf16[384,2048]{1,0:T(8,128)(2,1)} %scatter_custom_fusion) | data formatting | bytes 3145728 | tf_op jit(solution)/shard_map/reshape | solution.py:174
  52.1 3.3 %dynamic-slice_bitcast_fusion = bf16[64,1,3,2048]{3,2,1,0:T(4,128)(2,1)} fusion(bf16[64,1,6,2048]{3,2,0,1:T(8,128)(2,1)} %reshape.172, s32[]{:T(128)S(6)} %select_n.19), kind=kLoop, calls=%fused_computation.44 | loop fusion | bytes 1572868 | tf_op jit(solution)/shard_map/dynamic_slice | solution.py:177
  55.4 6.5 %all-to-all-start.1 = ((bf16[64,1,3,2048]{3,2,1,0:T(4,128)(2,1)}), bf16[64,1,3,2048]{3,2,1,0:T(4,128)(2,1)S(1)}, u32[]{:S(2)}, u32[]{:S(2)}) async-start(bf16[64,1,3,2048]{3,2,1,0:T(4,128)(2,1)} %dynamic-slice_bitcast_fusion), calls=%async_computation.1 | async-start | bytes 2097152 | tf_op jit(solution)/shard_map/all_to_all | solution.py:178
  61.9 2.1 %fusion.107 = f32[32,256]{1,0:T(8,128)} fusion(bf16[32,2048]{1,0:T(8,128)(2,1)S(1)} %add_convert_fusion, bf16[2048,256]{1,0:T(8,128)(2,1)} %param.44), kind=kOutput, calls=%fused_computation.145 | convolution fusion | flops 33554432 | bytes 1212416 | tf_op jit(solution)/shard_map/dot_general | solution.py:185
  64.1 2.9 %convolution_convert_fusion.1 = bf16[32,2048]{1,0:T(8,128)(2,1)} fusion(bf16[256,2048]{1,0:T(8,128)(2,1)} %param.46, bf16[32,2048]{1,0:T(8,128)(2,1)S(1)} %add_convert_fusion, bf16[2048,256]{1,0:T(8,128)(2,1)} %param.45, f32[32,256]{1,0:T(8,128)} %fusion.107), kind=kOutput, calls=%fused_computation.5 | convolution fusion | flops 67223552 | bytes 2392064 | tf_op jit(solution)/shard_map/dot_general | solution.py:188
  67.0 1.6 copy.99
  68.6 21.2 %all-to-all-done.1 = bf16[64,1,3,2048]{3,2,1,0:T(4,128)(2,1)S(1)} async-done(((bf16[64,1,3,2048]{3,2,1,0:T(4,128)(2,1)}), bf16[64,1,3,2048]{3,2,1,0:T(4,128)(2,1)S(1)}, u32[]{:S(2)}, u32[]{:S(2)}) %all-to-all-start.1) | async-done | bytes 786464 | tf_op jit(solution)/shard_map/all_to_all | solution.py:178
  89.7 0.6 copy.69
  90.3 0.2 broadcast_in_dim.14
  90.5 7.1 %all_to_all.30 = bf16[2,64,1,3,2048]{4,1,3,2,0:T(8,128)(2,1)S(1)} all-to-all(bf16[2,64,1,3,2048]{4,1,3,2,0:T(8,128)(2,1)S(1)} %broadcast_in_dim.14), channel_id=1, replica_groups=mesh['grp'=2,'ep'=64,'tp'=2] {'tp'}, dimensions={0} | all-to-all | bytes 3145728 | tf_op jit(solution)/shard_map/all_to_all | solution.py:26
  97.6 1.1 copy-done.1
  98.8 0.6 convolution_bitcast_fusion.1
  99.4 5.1 %convolution_convert_fusion = bf16[64,6,2048]{2,0,1:T(8,128)(2,1)} fusion(bf16[1,256,2048]{2,1,0:T(8,128)(2,1)} %param.43, bf16[64,6,2048]{2,0,1:T(8,128)(2,1)} %bitcast.164, bf16[1,2048,256]{2,1,0:T(8,128)(2,1)} %param.42, f32[64,1,6,256]{3,0,2,1:T(8,128)S(1)} %convolution_bitcast_fusion.1), kind=kOutput, calls=%fused_computation.4 | convolution fusion | flops 806682624 | bytes 5636096 | tf_op jit(solution)/shard_map/senf,efd->send/dot_general | solution.py:91
  104.5 1.6 copy.98
  106.1 5.8 %all_to_all.31 = bf16[2,64,1,6,1024]{4,1,3,2,0:T(8,128)(2,1)} all-to-all(bf16[2,64,1,6,1024]{4,1,3,2,0:T(8,128)(2,1)S(1)} %bitcast.165), channel_id=1, replica_groups=mesh['grp'=2,'ep'=64,'tp'=2] {'tp'}, dimensions={0} | all-to-all | bytes 3145728 | tf_op jit(solution)/shard_map/all_to_all | solution.py:20
  111.8 4.4 %all-to-all-start.5 = ((bf16[2,32,1024]{2,1,0:T(8,128)(2,1)}), bf16[2,32,1024]{2,1,0:T(8,128)(2,1)}, u32[]{:S(2)}, u32[]{:S(2)}) async-start(bf16[2,32,1024]{2,1,0:T(8,128)(2,1)} %bitcast.162), calls=%async_computation.5 | async-start | bytes 262144 | tf_op jit(solution)/shard_map/all_to_all | solution.py:20
  116.2 1.8 %reduce_sum.113 = bf16[64,6,1024]{2,0,1:T(8,128)(2,1)S(1)} reduce(bf16[2,64,1,6,1024]{4,1,3,2,0:T(8,128)(2,1)} %all_to_all.31, bf16[]{:T(256)} %constant.15.clone.1), dimensions={0,2}, to_apply=%region_6.7 | reduce | flops 393216 | bytes 2359298 | tf_op jit(solution)/shard_map/reduce_sum | solution.py:21
  118.1 1.4 copy.72
  119.6 8.6 %all-to-all-start.4 = ((bf16[64,1,6,1024]{3,2,1,0:T(8,128)(2,1)}), bf16[64,1,6,1024]{3,2,1,0:T(8,128)(2,1)}, u32[]{:S(2)}, u32[]{:S(2)}) async-start(bf16[64,1,6,1024]{3,2,1,0:T(8,128)(2,1)} %copy.72), calls=%async_computation.4 | async-start | bytes 2097152 | tf_op jit(solution)/shard_map/all_to_all | solution.py:96
  128.2 0.1 copy.73
  128.4 1.1 copy.75
  129.5 0.6 dynamic-slice
  130.7 1.6 reduce_sum.117
  132.3 0.6 fusion.28
  133.0 22.2 %all-to-all-done.4 = bf16[64,1,6,1024]{3,2,1,0:T(8,128)(2,1)} async-done(((bf16[64,1,6,1024]{3,2,1,0:T(8,128)(2,1)}), bf16[64,1,6,1024]{3,2,1,0:T(8,128)(2,1)}, u32[]{:S(2)}, u32[]{:S(2)}) %all-to-all-start.4) | async-done | bytes 786464 | tf_op jit(solution)/shard_map/all_to_all | solution.py:96
  155.2 1.4 reshape.179
  156.6 1.8 %gather_fusion = bf16[192,1024]{1,0:T(8,128)(2,1)} fusion(bf16[384,1024]{1,0:T(8,128)(2,1)S(1)} %reshape.179, s32[1024]{0:T(1024)S(1)} %pad_clamp_fusion), kind=kCustom, calls=%fused_computation | custom fusion | bytes 787200 | tf_op jit(solution)/shard_map/gather | solution.py:182
  158.4 1.1 reshape.182
  159.5 0.4 multiply_reduce_fusion
  159.9 4.7 %fusion.102 = (f32[32]{0:T(128)S(1)}, f32[32]{0:T(128)S(1)}, f32[32,1024]{1,0:T(8,128)S(1)}) fusion(bf16[1024,3072]{1,0:T(8,128)(2,1)} %all-gather.4.cloned.1.call-done, bf16[32,2048]{1,0:T(8,128)(2,1)S(1)} %add_convert_fusion, f32[32]{0:T(128)} %fusion.28, bf16[32,1024]{1,0:T(8,128)(2,1)} %reduce_sum.117, f32[32,1024]{1,0:T(8,128)S(1)} %multiply_reduce_fusion, ...), kind=kOutput, calls=%fused_computation.142 | convolution fusion | flops 201949120 | bytes 6816132 | tf_op jit(solution)/shard_map/dot_general | solution.py:105
  164.6 0.2 dynamic-update-slice
  164.9 0.2 dynamic-update-slice.1
  165.1 4.4 %all-reduce.3 = (f32[64]{0:T(128)S(1)}, f32[64]{0:T(128)S(1)}) all-reduce(f32[64]{0:T(128)S(1)} %dynamic-update-slice.1, f32[64]{0:T(128)S(1)} %dynamic-update-slice), channel_id=3, replica_groups=mesh['grp'=2,'ep'=64,'tp'=2] {'tp'}, use_global_device_ids=true, to_apply=%add.2 | all-reduce | flops 128 | bytes 1024
  169.5 0.1 reshape.199
  169.5 0.1 reshape.200
  169.7 0.7 add_convert_fusion.1
  (71 shorter events, 0.5 us)
Async XLA Ops:
  7.2 33.5 %copy-start = (bf16[512,2048]{1,0:T(8,128)(2,1)S(1)}, bf16[512,2048]{1,0:T(8,128)(2,1)}, u32[]{:S(2)}) copy-start(bf16[512,2048]{1,0:T(8,128)(2,1)} %param.36) | copy-start | bytes 6291460
  7.2 4.2 %copy-start.15 = (f32[16,64]{1,0:T(8,128)S(1)}, f32[16,64]{1,0:T(8,128)}, u32[]{:S(2)}) copy-start(f32[16,64]{1,0:T(8,128)} %param.29) | copy-start | bytes 12292
  7.2 4.2 %copy-start.14 = (f32[16,64]{1,0:T(8,128)S(1)}, f32[16,64]{1,0:T(8,128)}, u32[]{:S(2)}) copy-start(f32[16,64]{1,0:T(8,128)} %param.30) | copy-start | bytes 12292
  7.2 4.3 %copy-start.7 = (f32[2,32,16,64]{3,2,1,0:T(8,128)S(1)}, f32[2,32,16,64]{3,2,1,0:T(8,128)}, u32[]{:S(2)}) copy-start(f32[2,32,16,64]{3,2,1,0:T(8,128)} %param.27) | copy-start | bytes 786436
  7.2 4.4 %copy-start.9 = (f32[2,16,64,16]{2,3,1,0:T(8,128)S(1)}, f32[2,16,64,16]{2,3,1,0:T(8,128)}, u32[]{:S(2)}) copy-start(f32[2,16,64,16]{2,3,1,0:T(8,128)} %param.32) | copy-start | bytes 393220
  7.2 152.7 %all-gather.4.cloned.1.call-start = ((), (), s32[]{:S(2)}) async-start(), calls=%async_computation.6 | async-start | bytes 6389760 | tf_op jit(solution)/shard_map/all_gather | solution.py:45
  11.4 2.2 %copy-start.10 = (f32[2,16,64,16]{2,3,1,0:T(8,128)S(1)}, f32[2,16,64,16]{2,3,1,0:T(8,128)}, u32[]{:S(2)}) copy-start(f32[2,16,64,16]{2,3,1,0:T(8,128)} %param.32) | copy-start | bytes 393220
  11.6 3.2 %copy-start.8 = (f32[2,16,16,64]{3,2,1,0:T(8,128)S(1)}, f32[2,16,16,64]{3,2,1,0:T(8,128)}, u32[]{:S(2)}) copy-start(f32[2,16,16,64]{3,2,1,0:T(8,128)} %param.33) | copy-start | bytes 393220
  11.6 3.2 %copy-start.13 = (f32[16,16]{1,0:T(8,128)S(1)}, f32[16,16]{1,0:T(8,128)}, u32[]{:S(2)}) copy-start(f32[16,16]{1,0:T(8,128)} %param.34) | copy-start | bytes 3076
  12.1 28.6 %copy-start.5 = (bf16[512,512]{1,0:T(8,128)(2,1)S(1)}, bf16[512,512]{1,0:T(8,128)(2,1)}, u32[]{:S(2)}) copy-start(bf16[512,512]{1,0:T(8,128)(2,1)} %param.35) | copy-start | bytes 1572868
  12.1 28.6 %copy-start.6 = (bf16[32,2048]{1,0:T(8,128)(2,1)S(1)}, bf16[32,2048]{1,0:T(8,128)(2,1)}, u32[]{:S(2)}) copy-start(bf16[32,2048]{1,0:T(8,128)(2,1)} %param.26) | copy-start | bytes 393220
  14.0 0.7 copy-start.2
  16.0 24.7 %all-to-all-start = ((bf16[2,32,256]{2,1,0:T(8,128)(2,1)}), bf16[2,32,256]{2,1,0:T(8,128)(2,1)S(1)}, u32[]{:S(2)}, u32[]{:S(2)}) async-start(bf16[2,32,256]{2,1,0:T(8,128)(2,1)} %broadcast_in_dim.10), calls=%async_computation | async-start | bytes 65536 | tf_op jit(solution)/shard_map/all_to_all | solution.py:26
  40.7 1.0 copy-start.16
  40.8 1.0 copy-start.17
  41.9 1.3 copy-start.11
  44.6 7.5 %copy-start.21 = (s32[192,1]{0,1:T(1,128)}, s32[192,1]{0,1:T(1,128)S(1)}, u32[]{:S(2)}) copy-start(s32[192,1]{0,1:T(1,128)S(1)} %compare_select_fusion) | copy-start | bytes 2308
  55.4 34.3 %all-to-all-start.1 = ((bf16[64,1,3,2048]{3,2,1,0:T(4,128)(2,1)}), bf16[64,1,3,2048]{3,2,1,0:T(4,128)(2,1)S(1)}, u32[]{:S(2)}, u32[]{:S(2)}) async-start(bf16[64,1,3,2048]{3,2,1,0:T(4,128)(2,1)} %dynamic-slice_bitcast_fusion), calls=%async_computation.1 | async-start | bytes 2097152 | tf_op jit(solution)/shard_map/all_to_all | solution.py:178
  90.5 8.3 %copy-start.4 = (bf16[1,2048,256]{2,1,0:T(8,128)(2,1)S(1)}, bf16[1,2048,256]{2,1,0:T(8,128)(2,1)}, u32[]{:S(2)}) copy-start(bf16[1,2048,256]{2,1,0:T(8,128)(2,1)} %param.41) | copy-start | bytes 3145732
  97.6 1.1 copy-start.1
  111.8 7.7 %all-to-all-start.5 = ((bf16[2,32,1024]{2,1,0:T(8,128)(2,1)}), bf16[2,32,1024]{2,1,0:T(8,128)(2,1)}, u32[]{:S(2)}, u32[]{:S(2)}) async-start(bf16[2,32,1024]{2,1,0:T(8,128)(2,1)} %bitcast.162), calls=%async_computation.5 | async-start | bytes 262144 | tf_op jit(solution)/shard_map/all_to_all | solution.py:20
  118.1 10.1 %copy-start.12 = (f32[32,6]{0,1:T(8,128)S(1)}, f32[32,6]{0,1:T(8,128)}, u32[]{:S(2)}) copy-start(f32[32,6]{0,1:T(8,128)} %param.40) | copy-start | bytes 2308
  118.1 10.2 %copy-start.3 = (f32[32,16,64]{2,0,1:T(8,128)S(1)}, f32[32,16,64]{2,0,1:T(8,128)}, u32[]{:S(2)}) copy-start(f32[32,16,64]{2,0,1:T(8,128)} %copy-done.2) | copy-start | bytes 393220
  119.6 8.7 %copy-start.18 = (bf16[2048]{0:T(1024)(128)(2,1)S(1)}, bf16[2048]{0:T(1024)(128)(2,1)}, u32[]{:S(2)}) copy-start(bf16[2048]{0:T(1024)(128)(2,1)} %param.49) | copy-start | bytes 12292
  119.6 35.6 %all-to-all-start.4 = ((bf16[64,1,6,1024]{3,2,1,0:T(8,128)(2,1)}), bf16[64,1,6,1024]{3,2,1,0:T(8,128)(2,1)}, u32[]{:S(2)}, u32[]{:S(2)}) async-start(bf16[64,1,6,1024]{3,2,1,0:T(8,128)(2,1)} %copy.72), calls=%async_computation.4 | async-start | bytes 2097152 | tf_op jit(solution)/shard_map/all_to_all | solution.py:96
  128.1 1.3 copy-start.23
  128.2 4.1 %copy-start.22 = (s32[192,1]{0,1:T(1,128)S(1)}, s32[192,1]{0,1:T(1,128)}, u32[]{:S(2)}) copy-start(s32[192,1]{0,1:T(1,128)} %copy-done.21) | copy-start | bytes 2308
  159.9 9.8 %copy-start.19 = (f32[1024]{0:T(1024)S(1)}, f32[1024]{0:T(1024)}, u32[]{:S(2)}) copy-start(f32[1024]{0:T(1024)} %param.51) | copy-start | bytes 12292
  159.9 9.8 %copy-start.20 = (f32[1024]{0:T(1024)S(1)}, f32[1024]{0:T(1024)}, u32[]{:S(2)}) copy-start(f32[1024]{0:T(1024)} %param.50) | copy-start | bytes 12292
Sparse Core Ops, SparseCore 0:
  10.5 117.6 all-gather.3
where the time goes:
time: 178 us; the launch traced here: 177 us
  waiting for transfers between devices  44.5 us (25%)
  starting transfers between devices  43.2 us (24%)
  local copies, waits for them, and re-layouts  28.1 us (16%)
  matrix products  21.3 us (12%)
  blocking collectives  17.3 us (10%)
  between operations  15.2 us (9%)
  other arithmetic  7.59 us (4%)
    all_to_all x1, starting transfers between devices, from_everyone(): lax.all_to_all(jnp.broadcast_to(shard[None], (peers, *shard.shape)), axis...  23.7 us
    all_to_all x1, waiting for transfers between devices, finish_experts(): return lax.all_to_all(summed, 'ep', split_axis=0, concat_axis=0, tiled=True)  22.2 us
    all_to_all x1, waiting for transfers between devices, body(): lax.all_to_all(own_slots, 'ep', split_axis=0, concat_axis=0, tiled=True)  21.2 us
    all_to_all x1, starting transfers between devices, finish_experts(): return lax.all_to_all(summed, 'ep', split_axis=0, concat_axis=0, tiled=True)  8.57 us
    all_to_all x1, blocking collectives, from_everyone(): lax.all_to_all(jnp.broadcast_to(shard[None], (peers, *shard.shape)), axis...  7.11 us
    all_to_all x1, starting transfers between devices, body(): lax.all_to_all(own_slots, 'ep', split_axis=0, concat_axis=0, tiled=True)  6.51 us
    all_to_all x1, blocking collectives, sum_at_owner(): tiles = lax.all_to_all(cut_along(shard, dim, peers), axis, 0, 0, tiled=True)  5.77 us
    dot_general x1, matrix products, expert_terms(): jnp.einsum('senf,efd->send', hidden, down_weight, preferred_element_type=...  5.12 us
  transfers between devices with their start and end apart: 5, of which 3 were waited for; matrix products, arithmetic and copies ran while one was open for 27% of the time, Pallas kernels for 0%

commit v1 on v0

v1 whole, which is shorter than its diff:
```python
import functools
import math

import jax
import jax.numpy as jnp
from jax import lax
from jax.experimental import pallas as pl
from jax.experimental.pallas import tpu as pltpu
from jax.sharding import PartitionSpec as P

residual_alpha = 1.681792830507429
route_scale = 2.5
norm_eps = 1e-05
highest = lax.Precision.HIGHEST
MESH = pl.DeviceIdType.MESH
f32 = jnp.float32
bf16 = jnp.bfloat16
CHUNKS = 2


def state_update(
    inputs, ssm_state, decay_rate, frequency, step_log, input_map, output_map, skip_gain
):
    step_size = jnp.exp(step_log)[:, None]
    magnitude = jnp.exp(-decay_rate * step_size)
    rotation = frequency * step_size
    decay_re = magnitude * jnp.cos(rotation)
    decay_im = magnitude * jnp.sin(rotation)
    eigen_re = -decay_rate
    denominator = eigen_re * eigen_re + frequency * frequency
    factor_re = ((decay_re - 1.0) * eigen_re + decay_im * frequency) / denominator
    factor_im = (decay_im * eigen_re - (decay_re - 1.0) * frequency) / denominator
    drive_re = factor_re[..., None] * input_map[0] - factor_im[..., None] * input_map[1]
    drive_im = factor_re[..., None] * input_map[1] + factor_im[..., None] * input_map[0]
    pushed_re = jnp.einsum("gpm,tgm->tgp", drive_re, inputs, precision=highest)
    pushed_im = jnp.einsum("gpm,tgm->tgp", drive_im, inputs, precision=highest)
    new_re = decay_re * ssm_state[0] - decay_im * ssm_state[1] + pushed_re
    new_im = decay_re * ssm_state[1] + decay_im * ssm_state[0] + pushed_im
    response = (
        jnp.einsum("gmp,tgp->tgm", output_map[0], new_re, precision=highest)
        - jnp.einsum("gmp,tgp->tgm", output_map[1], new_im, precision=highest)
        + skip_gain * inputs
    )
    return (response, jnp.stack([new_re, new_im]))


def dot(a, b):
    return jnp.dot(a, b, preferred_element_type=f32)


def dot_t(a, b):
    return lax.dot_general(a, b, (((1,), (1,)), ((), ())), preferred_element_type=f32)


def iota(shape, dim):
    return lax.broadcasted_iota(jnp.int32, shape, dim).astype(f32)


def layer_kernel(
    side,
    cap,
    experts,
    act_ref,
    x_ref,
    ids_ref,
    rw_ref,
    gain_ref,
    shift_ref,
    din_ref,
    dout_ref,
    bgate_ref,
    fgain_ref,
    fshift_ref,
    glu_hbm,
    mix_hbm,
    ge_hbm,
    ue_hbm,
    de_hbm,
    gs_hbm,
    us_hbm,
    ds_hbm,
    out_ref,
    glu_v,
    mix_v,
    ge_v,
    ue_v,
    de_v,
    gs_v,
    us_v,
    ds_v,
    act_all,
    meta,
    din_all,
    dout_all,
    own_all,
    oth_all,
    x_send,
    x_recv,
    x_oth,
    y_send,
    y_oth,
    r_send,
    r_recv,
    s_send,
    s_recv,
    sh_send,
    sh_recv,
    st_send,
    st_recv,
    pick_v,
    mix_w,
    dense_v,
    load_sem,
    send_sem,
    recv_sem,
    tsend_sem,
    trecv_sem,
):
    rows, width = x_ref.shape
    half = width // 2
    chunks = own_all.shape[0]
    piece = half // chunks
    line_rows = side * rows
    slots = side * cap
    every = side * slots
    top_k = ids_ref.shape[1]
    core = lax.axis_index("tp")
    chip = lax.axis_index("ep")
    row, col = lax.div(chip, side), lax.rem(chip, side)
    p = (1 - core) * col + core * row
    q = (1 - core) * row + core * col

    def chip_at(pp, qq):
        return (1 - core) * (qq * side + pp) + core * (pp * side + qq)

    def line_peer(d):
        pp = lax.rem(p + d, side)
        return pp, {"ep": chip_at(pp, q), "tp": core}

    def cross_peer(d):
        qq = lax.rem(q + d, side)
        return qq, {"ep": chip_at(p, qq), "tp": core}

    partner = {"ep": chip, "tp": 1 - core}
    order = sorted(range(1, side), key=lambda d: -min(d, side - d))

    META, DIN, DOUT, OTH, OWN = 0, 1, 2, 3, 4
    XS, RS, SS = OWN + chunks, OWN + 2 * chunks, OWN + 3 * chunks

    def to_peer(kind, src, dst, place, device):
        me = q if kind in (DIN, DOUT) or XS <= kind < SS else p
        return pltpu.make_async_remote_copy(
            src_ref=src,
            dst_ref=dst,
            send_sem=send_sem.at[kind, place],
            recv_sem=recv_sem.at[kind, me],
            device_id=device,
            device_id_type=MESH,
        )

    def arrived(kind, dst, place):
        pltpu.make_async_remote_copy(
            src_ref=dst,
            dst_ref=dst,
            send_sem=send_sem.at[kind, place],
            recv_sem=recv_sem.at[kind, place],
            device_id=partner,
            device_id_type=MESH,
        ).wait_recv()

    def to_partner(kind, src, dst):
        return pltpu.make_async_remote_copy(
            src_ref=src,
            dst_ref=dst,
            send_sem=tsend_sem.at[kind],
            recv_sem=trecv_sem.at[kind],
            device_id=partner,
            device_id_type=MESH,
        )

    loads = [
        pltpu.make_async_copy(s, d, load_sem.at[i])
        for i, (s, d) in enumerate(
            [
                (glu_hbm, glu_v),
                (mix_hbm, mix_v),
                (gs_hbm, gs_v),
                (us_hbm, us_v),
                (ds_hbm, ds_v),
                (ge_hbm, ge_v),
                (ue_hbm, ue_v),
                (de_hbm, de_v),
            ]
        )
    ]
    for load in loads:
        load.start()

    barrier = pltpu.get_barrier_semaphore()
    pl.semaphore_signal(barrier, inc=1, device_id=partner, device_id_type=MESH)
    for d in range(1, side):
        for _, device in (line_peer(d), cross_peer(d)):
            pl.semaphore_signal(barrier, inc=1, device_id=device, device_id_type=MESH)
    pl.semaphore_wait(barrier, 2 * side - 1)

    sends = []

    def go(copy):
        copy.start()
        sends.append(copy)
        return copy

    act_copy = go(to_partner(0, act_ref, act_all.at[core]))
    act_all[core] = act_ref[...]

    lanes = meta.shape[3]
    ids, scores = ids_ref[...].astype(f32), rw_ref[...]
    scores = scores / jnp.sum(scores, axis=1, keepdims=True) * route_scale
    lane = iota((rows, lanes), 1)
    hits = jnp.zeros((rows, lanes), f32)
    share = jnp.zeros((rows, lanes), f32)
    for k in range(top_k):
        here = jnp.where(lane == ids[:, k : k + 1], 1.0, 0.0)
        hits += here
        share += here * scores[:, k : k + 1]
    earlier = jnp.where(iota((rows, rows), 1) < iota((rows, rows), 0), 1.0, 0.0)
    ranks = dot(earlier.astype(bf16), hits.astype(bf16))
    meta[p, 0] = jnp.where(hits > 0.5, ranks, -1.0).astype(bf16)
    meta[p, 1] = share.astype(bf16)
    din_all[q] = din_ref[...]
    dout_all[q] = dout_ref[...]
    for d in order:
        place, device = line_peer(d)
        go(to_peer(META, meta.at[p], meta.at[p], place, device))
    for d in order:
        place, device = cross_peer(d)
        go(to_peer(DIN, din_ref, din_all.at[q], place, device))
        go(to_peer(DOUT, dout_ref, dout_all.at[q], place, device))

    loads[0].wait()
    loads[1].wait()
    act_copy.wait_recv()
    channels = act_ref.shape[1]
    a0, a1 = act_all[0], act_all[1]
    gate = dot(a0, glu_v[:channels]) + dot(a1, glu_v[channels:])
    g0 = (a0.astype(f32) * jax.nn.sigmoid(gate[:, :channels])).astype(bf16)
    g1 = (a1.astype(f32) * jax.nn.sigmoid(gate[:, channels:])).astype(bf16)
    mixed = (dot(g0, mix_v[:channels]) + dot(g1, mix_v[channels:])).astype(bf16)
    values = residual_alpha * x_ref[...].astype(f32) + mixed.astype(f32)
    mean = jnp.mean(values, axis=1, keepdims=True)
    centred = values - mean
    variance = jnp.mean(centred * centred, axis=1, keepdims=True)
    normed = (centred * lax.rsqrt(variance + norm_eps) * gain_ref[...] + shift_ref[...]).astype(
        bf16
    )
    left, right = normed[:, :half], normed[:, half:]
    first = core == 0
    own = jnp.where(first, left, right)
    oth = jnp.where(first, right, left)
    for i in range(chunks):
        own_all[i, p] = own[:, i * piece : (i + 1) * piece]
    oth_all[p] = oth
    for i in range(chunks):
        for d in order:
            place, device = line_peer(d)
            go(to_peer(OWN + i, own_all.at[i, p], own_all.at[i, p], place, device))
    for d in order:
        place, device = line_peer(d)
        go(to_peer(OTH, oth_all.at[p], oth_all.at[p], place, device))

    for d in order:
        place, _ = line_peer(d)
        arrived(META, meta.at[place], place)
    lane = iota((1, every), 1)
    at_q = jnp.floor((lane + 0.5) / slots)
    at_p = jnp.floor((lane - at_q * slots + 0.5) / cap)
    at_rank = lane - at_q * slots - at_p * cap
    pf, cf = p.astype(f32), core.astype(f32)
    expert = (1.0 - cf) * (at_q * side + pf) + cf * (pf * side + at_q)
    spread = jnp.where(iota((lanes, every), 0) == expert, 1.0, 0.0).astype(bf16)
    codes = dot(meta[:, 0].reshape(line_rows, lanes), spread)
    shares = dot(meta[:, 1].reshape(line_rows, lanes), spread)
    block = jnp.floor((iota((line_rows, 1), 0) + 0.5) / rows)
    chosen = jnp.where((codes == at_rank) & (block == at_p), 1.0, 0.0)
    mix_w[...] = (chosen * shares).astype(bf16)
    pick_v[...] = chosen.T.astype(bf16)

    for load in loads[2:5]:
        load.wait()
    hidden = (jax.nn.silu(dot(normed, gs_v[...])) * dot(normed, us_v[...])).astype(bf16)
    base = core * half
    other = (1 - core) * half
    sh_send[...] = dot(hidden, ds_v[:, pl.ds(pl.multiple_of(other, 128), half)]).astype(bf16)
    shared_copy = go(to_partner(1, sh_send, sh_recv))
    shared_own = dot(hidden, ds_v[:, pl.ds(pl.multiple_of(base, 128), half)]).astype(bf16)

    for i in range(chunks):
        for d in order:
            place, _ = line_peer(d)
            arrived(OWN + i, own_all.at[i, place], place)
        picked = dot(pick_v[...], own_all[i].reshape(line_rows, piece)).astype(bf16)
        x_send[i] = picked.reshape(side, slots, piece)
        for d in order:
            place, device = cross_peer(d)
            go(to_peer(XS + i, x_send.at[i, place], x_recv.at[i, q], place, device))
        x_recv[i, q] = x_send[i, q]

    for d in order:
        place, _ = line_peer(d)
        arrived(OTH, oth_all.at[place], place)
    for d in order:
        place, _ = cross_peer(d)
        arrived(DIN, din_all.at[place], place)
        arrived(DOUT, dout_all.at[place], place)
    units = side * din_ref.shape[0]
    din = din_all[...].reshape(units, width)
    din_left, din_right = din[:, :half], din[:, half:]
    din_own = jnp.where(first, din_left, din_right)
    din_oth = jnp.where(first, din_right, din_left)
    bgate = jnp.broadcast_to(bgate_ref[...], (8, width))
    b_own = jnp.where(first, bgate[:, :half], bgate[:, half:])
    b_oth = jnp.where(first, bgate[:, half:], bgate[:, :half])
    oth_tok = oth_all[...].reshape(line_rows, half)
    before = dot_t(oth_tok, din_oth)
    gate = dot_t(oth_tok, b_oth)
    for i in range(chunks):
        tok = own_all[i].reshape(line_rows, piece)
        before += dot_t(tok, din_own[:, i * piece : (i + 1) * piece])
        gate += dot_t(tok, b_own[:, i * piece : (i + 1) * piece])
    dense_hidden = jax.nn.gelu(before).astype(bf16)
    branch = jax.nn.sigmoid(gate[:, :1])
    dense_v[...] = branch * dot(dense_hidden, dout_all[...].reshape(units, half))

    r0, r1 = iota((every, 1), 0), iota((1, every), 1)
    a = jnp.floor((r0 + 0.5) / slots)
    b = jnp.floor((r0 - a * slots + 0.5) / cap)
    swap = jnp.where(r1 == b * slots + a * cap + (r0 - a * slots - b * cap), 1.0, 0.0).astype(bf16)

    for i in range(chunks):
        for d in order:
            place, _ = cross_peer(d)
            arrived(XS + i, x_recv.at[i, place], place)
        go(to_partner(4 + i, x_recv.at[i], x_oth.at[i]))
    for load in loads[5:]:
        load.wait()
    units = ge_v.shape[1]
    gate = jnp.zeros((every, units), f32)
    up = jnp.zeros((every, units), f32)
    for i in range(chunks):
        tok = x_recv[i].reshape(every, piece)
        at = pl.ds(pl.multiple_of(base + i * piece, 128), piece)
        gate += dot(tok, ge_v[at])
        up += dot(tok, ue_v[at])
    for i in range(chunks):
        to_partner(4 + i, x_recv.at[i], x_oth.at[i]).wait_recv()
        tok = dot(swap, x_oth[i].reshape(every, piece)).astype(bf16)
        at = pl.ds(pl.multiple_of(other + i * piece, 128), piece)
        gate += dot(tok, ge_v[at])
        up += dot(tok, ue_v[at])
    hidden = (jax.nn.silu(gate) * up).astype(bf16)
    y_send[...] = dot(hidden, de_v[:, pl.ds(pl.multiple_of(other, 128), half)]).astype(bf16)
    y_copy = go(to_partner(2, y_send, y_oth))
    result = dot(hidden, de_v[:, pl.ds(pl.multiple_of(base, 128), half)])
    y_copy.wait_recv()
    for i in range(chunks):
        at = slice(i * piece, (i + 1) * piece)
        theirs = dot(swap, y_oth[:, at])
        r_send[i] = (result[:, at] + theirs).astype(bf16).reshape(side, slots, piece)
        for d in order:
            place, device = cross_peer(d)
            go(to_peer(RS + i, r_send.at[i, place], r_recv.at[i, q], place, device))
        r_recv[i, q] = r_send[i, q]

    for i in range(chunks):
        for d in order:
            place, _ = cross_peer(d)
            arrived(RS + i, r_recv.at[i, place], place)
        part = dot(mix_w[...], r_recv[i].reshape(every, piece))
        part += dense_v[:, i * piece : (i + 1) * piece]
        s_send[i] = part.astype(bf16).reshape(side, rows, piece)
        for d in order:
            place, device = line_peer(d)
            go(to_peer(SS + i, s_send.at[i, place], s_recv.at[i, p], place, device))
        s_recv[i, p] = s_send[i, p]

    shared_copy.wait_recv()
    shared = (shared_own.astype(f32) + sh_recv[...].astype(f32)).astype(bf16).astype(f32)
    skip = residual_alpha * own.astype(f32) + shared
    totals = []
    for i in range(chunks):
        for d in order:
            place, _ = line_peer(d)
            arrived(SS + i, s_recv.at[i, place], place)
        total = skip[:, i * piece : (i + 1) * piece]
        for j in range(side):
            total += s_recv[i, j].astype(f32)
        totals.append(total)
    row_sum = sum(jnp.sum(t, axis=1, keepdims=True) for t in totals)
    row_squares = sum(jnp.sum(t * t, axis=1, keepdims=True) for t in totals)
    st_send[...] = jnp.where(iota(st_send.shape, 1) < 0.5, row_sum, row_squares)
    st_copy = go(to_partner(3, st_send, st_recv))
    st_copy.wait_recv()
    mean = (row_sum + st_recv[:, 0:1]) / width
    variance = (row_squares + st_recv[:, 1:2]) / width - mean * mean
    scale = lax.rsqrt(variance + norm_eps)
    for i in range(chunks):
        at = slice(i * piece, (i + 1) * piece)
        out_ref[:, at] = ((totals[i] - mean) * scale * fgain_ref[:, at] + fshift_ref[:, at]).astype(
            bf16
        )
    for copy in sends:
        copy.wait_send()


def layer(side, cap, experts, vmem_args, hbm_args):
    rows, width = vmem_args[1].shape
    channels = vmem_args[0].shape[1]
    half = width // 2
    chunks = CHUNKS
    piece = half // chunks
    slots = side * cap
    every = side * slots
    lanes = -(-experts // 128) * 128
    din, dout = vmem_args[6], vmem_args[7]
    kinds = 4 + 4 * chunks
    V = pltpu.VMEM
    return pl.pallas_call(
        functools.partial(layer_kernel, side, cap, experts),
        out_shape=jax.ShapeDtypeStruct((rows, half), bf16),
        in_specs=[pl.BlockSpec(memory_space=pltpu.VMEM)] * len(vmem_args)
        + [pl.BlockSpec(memory_space=pl.ANY)] * len(hbm_args),
        out_specs=pl.BlockSpec(memory_space=pltpu.VMEM),
        scratch_shapes=[V(a.shape, bf16) for a in hbm_args]
        + [
            V((2, rows, channels), bf16),
            V((side, 2, rows, lanes), bf16),
            V((side, *din.shape), bf16),
            V((side, *dout.shape), bf16),
            V((chunks, side, rows, piece), bf16),
            V((side, rows, half), bf16),
            V((chunks, side, slots, piece), bf16),
            V((chunks, side, slots, piece), bf16),
            V((chunks, side, slots, piece), bf16),
            V((every, half), bf16),
            V((every, half), bf16),
            V((chunks, side, slots, piece), bf16),
            V((chunks, side, slots, piece), bf16),
            V((chunks, side, rows, piece), bf16),
            V((chunks, side, rows, piece), bf16),
            V((rows, half), bf16),
            V((rows, half), bf16),
            V((rows, 128), f32),
            V((rows, 128), f32),
            V((every, side * rows), bf16),
            V((side * rows, every), bf16),
            V((side * rows, half), f32),
            pltpu.SemaphoreType.DMA((len(hbm_args),)),
            pltpu.SemaphoreType.DMA((kinds, side)),
            pltpu.SemaphoreType.DMA((kinds, side)),
            pltpu.SemaphoreType.DMA((4 + chunks,)),
            pltpu.SemaphoreType.DMA((4 + chunks,)),
        ],
        compiler_params=pltpu.CompilerParams(
            collective_id=0, has_side_effects=True, vmem_limit_bytes=48 * 1024 * 1024
        ),
        name="layer",
    )(*vmem_args, *hbm_args)


def body(
    layer_input,
    ssm_state,
    w_input,
    decay_rate,
    frequency,
    step_log,
    input_map,
    output_map,
    skip_gain,
    glu_weight,
    mix_out,
    norm_gain,
    norm_shift,
    route_ids,
    route_weights,
    gate_expert,
    up_expert,
    down_expert,
    gate_shared,
    up_shared,
    down_shared,
    dense_in,
    dense_out,
    branch_gate,
    final_gain,
    final_shift,
):
    count_ep = lax.axis_size("ep")
    count_tp = lax.axis_size("tp")
    seq_rows, width = layer_input.shape
    local_groups, channels = skip_gain.shape
    projected = jnp.dot(layer_input, w_input, preferred_element_type=f32).astype(bf16)
    inputs = projected.astype(f32).reshape(seq_rows, local_groups, channels)
    response, new_state = state_update(
        inputs, ssm_state, decay_rate, frequency, step_log, input_map, output_map, skip_gain
    )
    activated = jax.nn.gelu(response.reshape(seq_rows, local_groups * channels)).astype(bf16)
    top_k = route_ids.shape[1]
    experts = gate_expert.shape[0] * count_ep
    cap = count_tp * max(1, min(seq_rows // count_tp, seq_rows * top_k // experts))
    side = math.isqrt(count_ep)
    layer_output = layer(
        side,
        cap,
        experts,
        [
            activated,
            layer_input,
            route_ids,
            route_weights,
            norm_gain[None],
            norm_shift[None],
            dense_in,
            dense_out,
            branch_gate[None],
            final_gain[None],
            final_shift[None],
        ],
        [
            glu_weight,
            mix_out,
            gate_expert[0],
            up_expert[0],
            down_expert[0],
            gate_shared,
            up_shared,
            down_shared,
        ],
    )
    return (layer_output, new_state)


def solution(mesh):
    placed = (
        P(("grp", "ep"), None),
        P(None, ("grp", "ep"), "tp", None),
        P(None, "tp"),
        P("tp", None),
        P("tp", None),
        P("tp"),
        P(None, "tp", None, None),
        P(None, "tp", None, None),
        P("tp", None),
        P(),
        P(),
        P(),
        P(),
        P(("grp", "ep"), None),
        P(("grp", "ep"), None),
        P("ep", None, "tp"),
        P("ep", None, "tp"),
        P("ep", "tp", None),
        P(None, "tp"),
        P(None, "tp"),
        P("tp", None),
        P("ep", None),
        P("ep", "tp"),
        P(),
        P("tp"),
        P("tp"),
    )
    return jax.shard_map(
        body,
        mesh=mesh,
        in_specs=placed,
        out_specs=(P(("grp", "ep"), "tp"), P(None, ("grp", "ep"), "tp", None)),
        check_vma=False,
    )
```

time: 178 us -> 103 us (0.58)
  the two profiles are of different devices: /device:TPU:513 before, /device:TPU:515 now
where the time goes in v1:
time: 103 us
  Pallas kernels  82.7 us (80%)
  local copies, waits for them, and re-layouts  11.1 us (11%)
  matrix products  7.22 us (7%)
    pallas_call x1, Pallas kernels, layer(): pl.pallas_call(functools.partial(layer_kernel, side, cap, experts), out_s...  82.7 us
    unnamed x50, local copies, waits for them, and re-layouts  7.42 us

profile of v1, /device:TPU:515, one launch (start us, length us, event | category | flops | bytes accessed | tf_op | source)
XLA Modules:
  0.0 102.9 jit_solution(11279686601840047962)
XLA Ops:
  0.6 0.0 copy-start
  0.6 0.7 exp.6
  1.4 0.8 add_divide_fusion
  2.2 1.9 %fusion.29 = (f32[1,32,16,64]{3,2,1,0:T(8,128)}, f32[1,32,16,64]{3,2,1,0:T(8,128)}) fusion(f32[2,32,16,64]{3,2,1,0:T(8,128)} %param.27), kind=kLoop, calls=%fused_computation.45 | loop fusion | bytes 524288 | tf_op jit(solution)/shard_map/slice | solution.py:37
  4.1 0.0 copy-start.19
  4.1 0.0 copy-done
  4.1 0.0 copy-start.20
  4.1 1.2 %convolution_convert_fusion = bf16[32,256]{1,0:T(8,128)(2,1)S(1)} fusion(bf16[32,2048]{1,0:T(8,128)(2,1)} %x_ref.1, bf16[2048,256]{1,0:T(8,128)(2,1)S(1)} %copy-done), kind=kOutput, calls=%fused_computation.7 | convolution fusion | flops 33562624 | bytes 1196032 | tf_op jit(solution)/shard_map/dot_general | solution.py:502
  5.3 0.0 copy-start.21
  5.3 0.0 copy-start.22
  5.3 0.0 copy-start.1
  5.3 0.0 copy-start.2
  5.4 0.0 copy-start.6
  5.4 0.0 copy-start.8
  5.4 0.0 copy-start.9
  5.4 0.0 copy-start.10
  5.4 0.0 copy-start.11
  5.4 0.0 copy-start.12
  5.4 0.0 copy-start.13
  5.4 0.1 copy.39
  5.6 0.0 copy-start.18
  5.6 1.7 %fusion = f32[32,16,64]{2,0,1:T(8,128)S(1)} fusion(bf16[32,16,16]{0,2,1:T(8,128)(2,1)S(1)} %bitcast.74, f32[1,32,16,64]{3,2,1,0:T(8,128)} %get-tuple-element.7, f32[1,32,16,64]{3,2,1,0:T(8,128)} %get-tuple-element.6, f32[16,64]{1,0:T(8,128)S(1)} %get-tuple-element.11, f32[16,64]{1,0:T(8,128)S(1)} %get-tuple-element.9, f32[2,16,64,16]{2,3,1,0:T(8,128)} %param.32, ...), kind=kOutput, calls=%fused_computation.1 | convolution fusion | flops 6471680 | bytes 557056 | tf_op jit(solution)/shard_map/gpm,tgm->tgp/dot_general | solution.py:36
  7.3 0.0 copy-start.16
  7.3 1.7 %fusion.1 = f32[32,16,64]{2,0,1:T(8,128)S(1)} fusion(bf16[32,16,16]{0,2,1:T(8,128)(2,1)S(1)} %bitcast.75, f32[1,32,16,64]{3,2,1,0:T(8,128)} %get-tuple-element.7, f32[1,32,16,64]{3,2,1,0:T(8,128)} %get-tuple-element.6, f32[16,64]{1,0:T(8,128)S(1)} %get-tuple-element.11, f32[16,64]{1,0:T(8,128)S(1)} %get-tuple-element.9, f32[2,16,64,16]{2,3,1,0:T(8,128)} %param.32, ...), kind=kOutput, calls=%fused_computation.3 | convolution fusion | flops 6471680 | bytes 557056 | tf_op jit(solution)/shard_map/gpm,tgm->tgp/dot_general | solution.py:35
  9.0 0.0 copy-start.14
  9.0 0.7 copy-done.14
  9.7 1.4 %fusion.5 = f32[16,32,16]{1,2,0:T(8,128)S(1)} fusion(f32[32,16,64]{2,0,1:T(8,128)S(1)} %fusion.1, f32[2,16,16,64]{3,2,1,0:T(8,128)} %param.33), kind=kOutput, calls=%fused_computation.12 | convolution fusion | flops 6291456 | bytes 294912 | tf_op jit(solution)/shard_map/gmp,tgp->tgm/dot_general | solution.py:40
  11.1 0.0 copy-done.16
  11.1 0.0 copy-done.19
  11.2 0.0 copy-done.18
  11.2 1.2 %fusion.3 = f32[32,16,16]{0,2,1:T(8,128)} fusion(f32[16,32,16]{1,2,0:T(8,128)S(1)} %fusion.5, f32[32,16,64]{2,0,1:T(8,128)S(1)} %fusion, bf16[32,16,16]{0,2,1:T(8,128)(2,1)S(1)} %bitcast.76, f32[2,16,16,64]{3,2,1,0:T(8,128)S(1)} %copy-done.18, f32[16,16]{1,0:T(8,128)S(1)} %copy-done.19), kind=kOutput, calls=%fused_computation.6 | convolution fusion | flops 6324224 | bytes 630784 | tf_op jit(solution)/shard_map/gmp,tgp->tgm/dot_general | solution.py:41
  12.3 1.0 copy.44
  13.4 0.0 copy-done.20
  13.4 0.1 copy.45.ids_ref
  13.5 0.0 copy-done.21
  13.5 0.1 copy.46.rw_ref
  13.5 0.0 copy-done.22
  13.6 0.0 copy-done.1
  13.6 0.0 copy-done.2
  13.6 0.0 copy-done.6
  13.6 0.0 copy-done.8
  13.6 0.0 copy-done.9
  13.6 0.0 copy-done.10
  13.6 0.0 copy-done.11
  13.6 0.0 copy-done.12
  13.6 0.0 copy-done.13
  13.6 0.0 copy-start.3
  13.7 1.2 %copy-done.3 = bf16[1,256,2048]{2,1,0:T(8,128)(2,1)S(1)} copy-done((bf16[1,256,2048]{2,1,0:T(8,128)(2,1)S(1)}, bf16[1,256,2048]{2,1,0:T(8,128)(2,1)}, u32[]{:S(2)}) %copy-start.3) | copy-done | bytes 1048600
  14.9 0.0 copy-start.4
  14.9 1.2 %copy-done.4 = bf16[2048,256]{1,0:T(8,128)(2,1)S(1)} copy-done((bf16[2048,256]{1,0:T(8,128)(2,1)S(1)}, bf16[2048,256]{1,0:T(8,128)(2,1)}, u32[]{:S(2)}) %copy-start.4) | copy-done | bytes 1048600
  16.1 0.0 copy-start.5
  16.1 1.2 %copy-done.5 = bf16[2048,256]{1,0:T(8,128)(2,1)S(1)} copy-done((bf16[2048,256]{1,0:T(8,128)(2,1)S(1)}, bf16[2048,256]{1,0:T(8,128)(2,1)}, u32[]{:S(2)}) %copy-start.5) | copy-done | bytes 1048600
  17.3 0.0 copy-start.7
  17.3 1.0 %copy-done.7 = bf16[512,512]{1,0:T(8,128)(2,1)S(1)} copy-done((bf16[512,512]{1,0:T(8,128)(2,1)S(1)}, bf16[512,512]{1,0:T(8,128)(2,1)}, u32[]{:S(2)}) %copy-start.7) | copy-done | bytes 524312
  18.4 0.0 copy-start.15
  18.4 0.0 copy-start.17
  18.4 82.7 %layer.1 = bf16[32,1024]{1,0:T(8,128)(2,1)S(1)} custom-call(bf16[32,256]{1,0:T(8,128)(2,1)S(1)} %fusion.28.act_ref, bf16[32,2048]{1,0:T(8,128)(2,1)S(1)} %copy-done.6, s32[32,6]{1,0:T(8,128)S(1)} %copy.45.ids_ref, f32[32,6]{1,0:T(8,128)S(1)} %copy.46.rw_ref, f32[1,2048]{1,0:T(1,128)S(1)} %bitcast.68, f32[1,2048]{1,0:T(1,128)S(1)} %bitcast.69, ...), custom_call_target="tpu_custom_call" | custom-call | tf_op jit(solution)/shard_map/layer/pallas_call | solution.py:427
  101.1 0.0 copy-done.15
  101.1 0.0 copy-done.17
  101.1 1.1 %copy.47 = f32[2,32,16,64]{3,2,1,0:T(8,128)} copy(f32[2,32,16,64]{3,1,2,0:T(8,128)S(1)} %pad_maximum_fusion) | data formatting | bytes 524288
  102.2 0.6 copy.61
  (3 shorter events, 0.1 us)
Async XLA Ops:
  0.6 3.5 %copy-start = (bf16[2048,256]{1,0:T(8,128)(2,1)S(1)}, bf16[2048,256]{1,0:T(8,128)(2,1)}, u32[]{:S(2)}) copy-start(bf16[2048,256]{1,0:T(8,128)(2,1)} %param.28) | copy-start | bytes 3145732
  4.1 7.0 %copy-start.19 = (f32[16,16]{1,0:T(8,128)S(1)}, f32[16,16]{1,0:T(8,128)}, u32[]{:S(2)}) copy-start(f32[16,16]{1,0:T(8,128)} %param.34) | copy-start | bytes 3076
  4.1 9.3 %copy-start.20 = (s32[32,6]{0,1:T(8,128)S(1)}, s32[32,6]{0,1:T(8,128)}, u32[]{:S(2)}) copy-start(s32[32,6]{0,1:T(8,128)} %param.39) | copy-start | bytes 2308
  5.3 8.1 %copy-start.21 = (f32[32,6]{0,1:T(8,128)S(1)}, f32[32,6]{0,1:T(8,128)}, u32[]{:S(2)}) copy-start(f32[32,6]{0,1:T(8,128)} %param.40) | copy-start | bytes 2308
  5.3 8.2 %copy-start.22 = (bf16[2048]{0:T(1024)(128)(2,1)S(1)}, bf16[2048]{0:T(1024)(128)(2,1)}, u32[]{:S(2)}) copy-start(bf16[2048]{0:T(1024)(128)(2,1)} %param.49) | copy-start | bytes 12292
  5.3 8.2 %copy-start.1 = (bf16[1,2048,256]{2,1,0:T(8,128)(2,1)S(1)}, bf16[1,2048,256]{2,1,0:T(8,128)(2,1)}, u32[]{:S(2)}) copy-start(bf16[1,2048,256]{2,1,0:T(8,128)(2,1)} %param.41) | copy-start | bytes 3145732
  5.3 8.2 %copy-start.2 = (bf16[1,2048,256]{2,1,0:T(8,128)(2,1)S(1)}, bf16[1,2048,256]{2,1,0:T(8,128)(2,1)}, u32[]{:S(2)}) copy-start(bf16[1,2048,256]{2,1,0:T(8,128)(2,1)} %param.42) | copy-start | bytes 3145732
  5.4 8.2 %copy-start.6 = (bf16[32,2048]{1,0:T(8,128)(2,1)S(1)}, bf16[32,2048]{1,0:T(8,128)(2,1)}, u32[]{:S(2)}) copy-start(bf16[32,2048]{1,0:T(8,128)(2,1)} %x_ref.1) | copy-start | bytes 393220
  5.4 8.2 %copy-start.8 = (bf16[16,2048]{1,0:T(8,128)(2,1)S(1)}, bf16[16,2048]{1,0:T(8,128)(2,1)}, u32[]{:S(2)}) copy-start(bf16[16,2048]{1,0:T(8,128)(2,1)} %din_ref.1) | copy-start | bytes 196612
  5.4 8.2 %copy-start.9 = (bf16[16,1024]{1,0:T(8,128)(2,1)S(1)}, bf16[16,1024]{1,0:T(8,128)(2,1)}, u32[]{:S(2)}) copy-start(bf16[16,1024]{1,0:T(8,128)(2,1)} %dout_ref.1) | copy-start | bytes 98308
  5.4 8.2 %copy-start.10 = (f32[2048]{0:T(1024)S(1)}, f32[2048]{0:T(1024)}, u32[]{:S(2)}) copy-start(f32[2048]{0:T(1024)} %param.37) | copy-start | bytes 24580
  5.4 8.2 %copy-start.11 = (f32[2048]{0:T(1024)S(1)}, f32[2048]{0:T(1024)}, u32[]{:S(2)}) copy-start(f32[2048]{0:T(1024)} %param.38) | copy-start | bytes 24580
  5.4 8.2 %copy-start.12 = (f32[1024]{0:T(1024)S(1)}, f32[1024]{0:T(1024)}, u32[]{:S(2)}) copy-start(f32[1024]{0:T(1024)} %param.50) | copy-start | bytes 12292
  5.4 8.2 %copy-start.13 = (f32[1024]{0:T(1024)S(1)}, f32[1024]{0:T(1024)}, u32[]{:S(2)}) copy-start(f32[1024]{0:T(1024)} %param.51) | copy-start | bytes 12292
  5.6 5.6 %copy-start.18 = (f32[2,16,16,64]{3,2,1,0:T(8,128)S(1)}, f32[2,16,16,64]{3,2,1,0:T(8,128)}, u32[]{:S(2)}) copy-start(f32[2,16,16,64]{3,2,1,0:T(8,128)} %param.33) | copy-start | bytes 393220
  7.3 3.8 %copy-start.16 = (f32[32,16,64]{2,0,1:T(8,128)}, f32[32,16,64]{2,0,1:T(8,128)S(1)}, u32[]{:S(2)}) copy-start(f32[32,16,64]{2,0,1:T(8,128)S(1)} %fusion) | copy-start | bytes 393220
  9.0 0.7 copy-start.14
  13.6 1.2 %copy-start.3 = (bf16[1,256,2048]{2,1,0:T(8,128)(2,1)S(1)}, bf16[1,256,2048]{2,1,0:T(8,128)(2,1)}, u32[]{:S(2)}) copy-start(bf16[1,256,2048]{2,1,0:T(8,128)(2,1)} %param.43) | copy-start | bytes 3145732
  14.9 1.2 %copy-start.4 = (bf16[2048,256]{1,0:T(8,128)(2,1)S(1)}, bf16[2048,256]{1,0:T(8,128)(2,1)}, u32[]{:S(2)}) copy-start(bf16[2048,256]{1,0:T(8,128)(2,1)} %gs_hbm.1) | copy-start | bytes 3145732
  16.1 1.2 %copy-start.5 = (bf16[2048,256]{1,0:T(8,128)(2,1)S(1)}, bf16[2048,256]{1,0:T(8,128)(2,1)}, u32[]{:S(2)}) copy-start(bf16[2048,256]{1,0:T(8,128)(2,1)} %us_hbm.1) | copy-start | bytes 3145732
  17.3 1.0 %copy-start.7 = (bf16[512,512]{1,0:T(8,128)(2,1)S(1)}, bf16[512,512]{1,0:T(8,128)(2,1)}, u32[]{:S(2)}) copy-start(bf16[512,512]{1,0:T(8,128)(2,1)} %glu_hbm.1) | copy-start | bytes 1572868
  18.4 82.7 %copy-start.15 = (f32[32,16,64]{2,0,1:T(8,128)S(1)}, f32[32,16,64]{2,0,1:T(8,128)}, u32[]{:S(2)}) copy-start(f32[32,16,64]{2,0,1:T(8,128)} %copy-done.14) | copy-start | bytes 393220
  18.4 82.7 %copy-start.17 = (f32[32,16,64]{2,0,1:T(8,128)S(1)}, f32[32,16,64]{2,0,1:T(8,128)}, u32[]{:S(2)}) copy-start(f32[32,16,64]{2,0,1:T(8,128)} %copy-done.16) | copy-start | bytes 393220

commit v2 on v1

v2 whole, which is shorter than its diff:
```python
import functools
import math

import jax
import jax.numpy as jnp
from jax import lax
from jax.experimental import pallas as pl
from jax.experimental.pallas import tpu as pltpu
from jax.sharding import PartitionSpec as P

residual_alpha = 1.681792830507429
route_scale = 2.5
norm_eps = 1e-05
highest = lax.Precision.HIGHEST
MESH = pl.DeviceIdType.MESH
f32 = jnp.float32
bf16 = jnp.bfloat16
CHUNKS = 2
VMEM_BYTES = 64 * 1024 * 1024 - 1024 * 1024


def dot(a, b):
    return jnp.dot(a, b, preferred_element_type=f32)


def dot_t(a, b):
    return lax.dot_general(a, b, (((1,), (1,)), ((), ())), preferred_element_type=f32)


def iota(shape, dim):
    return lax.broadcasted_iota(jnp.int32, shape, dim).astype(f32)


def halves(a):
    high = a.astype(bf16)
    return high, (a - high.astype(f32)).astype(bf16)


def layer_kernel(side, cap, names, *refs):
    count = len(names)
    hbm = refs[:count]
    out_ref, new_ref = refs[count : count + 2]
    local = dict(zip(names, refs[count + 2 :]))
    rest = refs[2 * count + 2 :]
    layer_steps(side, cap, names, hbm, local, out_ref, new_ref, *rest)


def layer_steps(
    side,
    cap,
    names,
    hbm,
    local,
    out_ref,
    new_ref,
    drive_v,
    omap_v,
    act_send,
    act_all,
    meta,
    din_all,
    dout_all,
    own_all,
    oth_all,
    x_send,
    x_recv,
    x_oth,
    y_send,
    y_oth,
    r_send,
    r_recv,
    s_send,
    s_recv,
    sh_send,
    sh_recv,
    st_send,
    st_recv,
    pick_v,
    mix_w,
    dense_v,
    load_sem,
    send_sem,
    recv_sem,
    tsend_sem,
    trecv_sem,
):
    x_ref, din_ref, dout_ref = local["x"], local["din"], local["dout"]
    rows, width = x_ref.shape
    half = width // 2
    chunks = own_all.shape[0]
    piece = half // chunks
    line_rows = side * rows
    slots = side * cap
    every = side * slots
    core = lax.axis_index("tp")
    chip = lax.axis_index("ep")
    row, col = lax.div(chip, side), lax.rem(chip, side)
    p = (1 - core) * col + core * row
    q = (1 - core) * row + core * col

    def chip_at(pp, qq):
        return (1 - core) * (qq * side + pp) + core * (pp * side + qq)

    def line_peer(d):
        pp = lax.rem(p + d, side)
        return pp, {"ep": chip_at(pp, q), "tp": core}

    def cross_peer(d):
        qq = lax.rem(q + d, side)
        return qq, {"ep": chip_at(p, qq), "tp": core}

    partner = {"ep": chip, "tp": 1 - core}
    order = sorted(range(1, side), key=lambda d: -min(d, side - d))

    META, DIN, DOUT, OTH, OWN = 0, 1, 2, 3, 4
    XS, RS, SS = OWN + chunks, OWN + 2 * chunks, OWN + 3 * chunks

    def to_peer(kind, src, dst, place, device):
        me = q if kind in (DIN, DOUT) or XS <= kind < SS else p
        return pltpu.make_async_remote_copy(
            src_ref=src,
            dst_ref=dst,
            send_sem=send_sem.at[kind, place],
            recv_sem=recv_sem.at[kind, me],
            device_id=device,
            device_id_type=MESH,
        )

    def arrived(kind, dst, place):
        pltpu.make_async_remote_copy(
            src_ref=dst,
            dst_ref=dst,
            send_sem=send_sem.at[kind, place],
            recv_sem=recv_sem.at[kind, place],
            device_id=partner,
            device_id_type=MESH,
        ).wait_recv()

    def to_partner(kind, src, dst):
        return pltpu.make_async_remote_copy(
            src_ref=src,
            dst_ref=dst,
            send_sem=tsend_sem.at[kind],
            recv_sem=trecv_sem.at[kind],
            device_id=partner,
            device_id_type=MESH,
        )

    loads = {
        name: pltpu.make_async_copy(src, local[name], load_sem.at[i])
        for i, (name, src) in enumerate(zip(names, hbm))
    }
    for load in loads.values():
        load.start()

    def loaded(*wanted):
        for name in wanted:
            loads[name].wait()

    barrier = pltpu.get_barrier_semaphore()
    pl.semaphore_signal(barrier, inc=1, device_id=partner, device_id_type=MESH)
    for d in range(1, side):
        for _, device in (line_peer(d), cross_peer(d)):
            pl.semaphore_signal(barrier, inc=1, device_id=device, device_id_type=MESH)

    lanes = meta.shape[3]
    loaded("ids", "scores")
    ids, scores = local["ids"][...].astype(f32), local["scores"][...]
    scores = scores / jnp.sum(scores, axis=0, keepdims=True) * route_scale
    eye = iota((rows, rows), 0) == iota((rows, rows), 1)
    lane = iota((rows, lanes), 1)
    hits = jnp.zeros((rows, lanes), f32)
    share = jnp.zeros((rows, lanes), f32)
    for k in range(ids.shape[0]):
        name = jnp.sum(jnp.where(eye, ids[k : k + 1], 0.0), axis=1, keepdims=True)
        score = jnp.sum(jnp.where(eye, scores[k : k + 1], 0.0), axis=1, keepdims=True)
        here = jnp.where(lane == name, 1.0, 0.0)
        hits += here
        share += here * score
    earlier = jnp.where(iota((rows, rows), 1) < iota((rows, rows), 0), 1.0, 0.0)
    ranks = dot(earlier.astype(bf16), hits.astype(bf16))
    meta[p, 0] = jnp.where(hits > 0.5, ranks, -1.0).astype(bf16)
    meta[p, 1] = share.astype(bf16)

    groups, states = local["rate"].shape
    members = local["skip"].shape[1]
    channels = groups * members
    pair = 2 * states
    drive_v[...] = jnp.zeros_like(drive_v)
    omap_v[...] = jnp.zeros_like(omap_v)
    loaded("rate", "freq", "step", "imap", "omap", "skip")
    rate, freq = local["rate"][...], local["freq"][...]
    eye = iota((groups, groups), 0) == iota((groups, groups), 1)
    step = jnp.exp(jnp.sum(jnp.where(eye, local["step"][...], 0.0), axis=1, keepdims=True))
    magnitude = jnp.exp(-rate * step)
    angle = freq * step
    decay_re, decay_im = magnitude * jnp.cos(angle), magnitude * jnp.sin(angle)
    denominator = rate * rate + freq * freq
    factor_re = ((decay_re - 1.0) * -rate + decay_im * freq) / denominator
    factor_im = (decay_im * -rate - (decay_re - 1.0) * freq) / denominator
    same = jnp.concatenate([decay_re, decay_re], axis=1)
    cross = jnp.concatenate([-decay_im, decay_im], axis=1)
    for g in range(groups):
        fr, fi = factor_re[g : g + 1], factor_im[g : g + 1]
        m0, m1 = local["imap"][0, g], local["imap"][1, g]
        drive = jnp.concatenate([fr * m0 - fi * m1, fr * m1 + fi * m0], axis=1)
        out = jnp.concatenate([local["omap"][0, g], -local["omap"][1, g]], axis=1)
        at, lanes_at = slice(g * members, (g + 1) * members), slice(g * pair, (g + 1) * pair)
        drive_v[0, at, lanes_at], drive_v[1, at, lanes_at] = halves(drive)
        omap_v[0, at, lanes_at], omap_v[1, at, lanes_at] = halves(out)
    tile = jnp.where(
        iota((members, channels), 0)
        == iota((members, channels), 1)
        - jnp.floor((iota((members, channels), 1) + 0.5) / members) * members,
        1.0,
        0.0,
    )
    skip = jnp.dot(local["skip"][...], tile, preferred_element_type=f32, precision=highest)
    in_group = jnp.floor((iota((groups, channels), 1) + 0.5) / members) == iota(
        (groups, channels), 0
    )
    skip = jnp.sum(jnp.where(in_group, skip, 0.0), axis=0, keepdims=True)
    loaded("x", "win")
    projected = dot(x_ref[...], local["win"][...]).astype(bf16)
    pushed = dot(projected, drive_v[0]) + dot(projected, drive_v[1])
    loaded("state")
    response = skip * projected.astype(f32)
    highs, lows = [], []
    for g in range(groups):
        old = jnp.concatenate(
            [
                local["state"][pl.ds(g, rows, stride=groups)],
                local["state"][pl.ds(rows * groups + g, rows, stride=groups)],
            ],
            axis=1,
        )
        turned = jnp.concatenate([old[:, states:], old[:, :states]], axis=1)
        new = same[g : g + 1] * old + cross[g : g + 1] * turned
        new += pushed[:, g * pair : (g + 1) * pair]
        new_ref[pl.ds(g, rows, stride=groups)] = new[:, :states]
        new_ref[pl.ds(rows * groups + g, rows, stride=groups)] = new[:, states:]
        high, low = halves(new)
        highs.append(high)
        lows.append(low)
    high, low = jnp.concatenate(highs, axis=1), jnp.concatenate(lows, axis=1)
    response += dot_t(high, omap_v[0]) + dot_t(high, omap_v[1]) + dot_t(low, omap_v[0])
    act_send[...] = jax.nn.gelu(response).astype(bf16)

    pl.semaphore_wait(barrier, 2 * side - 1)
    sends = []

    def go(copy):
        copy.start()
        sends.append(copy)
        return copy

    act_copy = go(to_partner(0, act_send, act_all.at[core]))
    act_all[core] = act_send[...]
    loaded("din", "dout")
    din_all[q] = din_ref[...]
    dout_all[q] = dout_ref[...]
    for d in order:
        place, device = line_peer(d)
        go(to_peer(META, meta.at[p], meta.at[p], place, device))
    for d in order:
        place, device = cross_peer(d)
        go(to_peer(DIN, din_ref, din_all.at[q], place, device))
        go(to_peer(DOUT, dout_ref, dout_all.at[q], place, device))

    loaded("glu", "mix", "gain", "shift")
    glu_v, mix_v = local["glu"], local["mix"]
    act_copy.wait_recv()
    a0, a1 = act_all[0], act_all[1]
    gate = dot(a0, glu_v[:channels]) + dot(a1, glu_v[channels:])
    g0 = (a0.astype(f32) * jax.nn.sigmoid(gate[:, :channels])).astype(bf16)
    g1 = (a1.astype(f32) * jax.nn.sigmoid(gate[:, channels:])).astype(bf16)
    mixed = (dot(g0, mix_v[:channels]) + dot(g1, mix_v[channels:])).astype(bf16)
    values = residual_alpha * x_ref[...].astype(f32) + mixed.astype(f32)
    mean = jnp.mean(values, axis=1, keepdims=True)
    centred = values - mean
    variance = jnp.mean(centred * centred, axis=1, keepdims=True)
    normed = (centred * lax.rsqrt(variance + norm_eps) * local["gain"][...] + local["shift"][...]).astype(
        bf16
    )
    left, right = normed[:, :half], normed[:, half:]
    first = core == 0
    own = jnp.where(first, left, right)
    oth = jnp.where(first, right, left)
    for i in range(chunks):
        own_all[i, p] = own[:, i * piece : (i + 1) * piece]
    oth_all[p] = oth
    for i in range(chunks):
        for d in order:
            place, device = line_peer(d)
            go(to_peer(OWN + i, own_all.at[i, p], own_all.at[i, p], place, device))

    for d in order:
        place, _ = line_peer(d)
        arrived(META, meta.at[place], place)
    lane = iota((1, every), 1)
    at_q = jnp.floor((lane + 0.5) / slots)
    at_p = jnp.floor((lane - at_q * slots + 0.5) / cap)
    at_rank = lane - at_q * slots - at_p * cap
    pf, cf = p.astype(f32), core.astype(f32)
    expert = (1.0 - cf) * (at_q * side + pf) + cf * (pf * side + at_q)
    spread = jnp.where(iota((lanes, every), 0) == expert, 1.0, 0.0).astype(bf16)
    codes = dot(meta[:, 0].reshape(line_rows, lanes), spread)
    shares = dot(meta[:, 1].reshape(line_rows, lanes), spread)
    block = jnp.floor((iota((line_rows, 1), 0) + 0.5) / rows)
    chosen = jnp.where((codes == at_rank) & (block == at_p), 1.0, 0.0)
    mix_w[...] = (chosen * shares).astype(bf16)
    pick_v[...] = chosen.T.astype(bf16)

    loaded("gs", "us", "ds")
    gs_v, us_v, ds_v = local["gs"], local["us"], local["ds"]
    hidden = (jax.nn.silu(dot(normed, gs_v[...])) * dot(normed, us_v[...])).astype(bf16)
    base = core * half
    other = (1 - core) * half
    sh_send[...] = dot(hidden, ds_v[:, pl.ds(pl.multiple_of(other, 128), half)]).astype(bf16)
    shared_copy = go(to_partner(1, sh_send, sh_recv))
    shared_own = dot(hidden, ds_v[:, pl.ds(pl.multiple_of(base, 128), half)]).astype(bf16)

    for i in range(chunks):
        for d in order:
            place, _ = line_peer(d)
            arrived(OWN + i, own_all.at[i, place], place)
        picked = dot(pick_v[...], own_all[i].reshape(line_rows, piece)).astype(bf16)
        x_send[i] = picked.reshape(side, slots, piece)
        for d in order:
            place, device = cross_peer(d)
            go(to_peer(XS + i, x_send.at[i, place], x_recv.at[i, q], place, device))
        x_recv[i, q] = x_send[i, q]

    r0, r1 = iota((every, 1), 0), iota((1, every), 1)
    a = jnp.floor((r0 + 0.5) / slots)
    b = jnp.floor((r0 - a * slots + 0.5) / cap)
    swap = jnp.where(r1 == b * slots + a * cap + (r0 - a * slots - b * cap), 1.0, 0.0).astype(bf16)

    for i in range(chunks):
        for d in order:
            place, _ = cross_peer(d)
            arrived(XS + i, x_recv.at[i, place], place)
        go(to_partner(4 + i, x_recv.at[i], x_oth.at[i]))
    for d in order:
        place, device = line_peer(d)
        go(to_peer(OTH, oth_all.at[p], oth_all.at[p], place, device))
    loaded("ge", "ue", "de")
    ge_v, ue_v, de_v = local["ge"], local["ue"], local["de"]
    units = ge_v.shape[1]
    gate = jnp.zeros((every, units), f32)
    up = jnp.zeros((every, units), f32)
    for i in range(chunks):
        tok = x_recv[i].reshape(every, piece)
        at = pl.ds(pl.multiple_of(base + i * piece, 128), piece)
        gate += dot(tok, ge_v[at])
        up += dot(tok, ue_v[at])
    for i in range(chunks):
        to_partner(4 + i, x_recv.at[i], x_oth.at[i]).wait_recv()
        tok = dot(swap, x_oth[i].reshape(every, piece)).astype(bf16)
        at = pl.ds(pl.multiple_of(other + i * piece, 128), piece)
        gate += dot(tok, ge_v[at])
        up += dot(tok, ue_v[at])
    hidden = (jax.nn.silu(gate) * up).astype(bf16)
    y_send[...] = dot(hidden, de_v[:, pl.ds(pl.multiple_of(other, 128), half)]).astype(bf16)
    y_copy = go(to_partner(2, y_send, y_oth))
    result = dot(hidden, de_v[:, pl.ds(pl.multiple_of(base, 128), half)])
    y_copy.wait_recv()
    for i in range(chunks):
        at = slice(i * piece, (i + 1) * piece)
        theirs = dot(swap, y_oth[:, at])
        r_send[i] = (result[:, at] + theirs).astype(bf16).reshape(side, slots, piece)
        for d in order:
            place, device = cross_peer(d)
            go(to_peer(RS + i, r_send.at[i, place], r_recv.at[i, q], place, device))
        r_recv[i, q] = r_send[i, q]

    for d in order:
        place, _ = line_peer(d)
        arrived(OTH, oth_all.at[place], place)
    for d in order:
        place, _ = cross_peer(d)
        arrived(DIN, din_all.at[place], place)
        arrived(DOUT, dout_all.at[place], place)
    units = side * din_ref.shape[0]
    din = din_all[...].reshape(units, width)
    din_left, din_right = din[:, :half], din[:, half:]
    din_own = jnp.where(first, din_left, din_right)
    din_oth = jnp.where(first, din_right, din_left)
    loaded("bgate")
    bgate = jnp.broadcast_to(local["bgate"][...], (8, width))
    b_own = jnp.where(first, bgate[:, :half], bgate[:, half:])
    b_oth = jnp.where(first, bgate[:, half:], bgate[:, :half])
    oth_tok = oth_all[...].reshape(line_rows, half)
    before = dot_t(oth_tok, din_oth)
    gate = dot_t(oth_tok, b_oth)
    for i in range(chunks):
        tok = own_all[i].reshape(line_rows, piece)
        before += dot_t(tok, din_own[:, i * piece : (i + 1) * piece])
        gate += dot_t(tok, b_own[:, i * piece : (i + 1) * piece])
    dense_hidden = jax.nn.gelu(before).astype(bf16)
    branch = jax.nn.sigmoid(gate[:, :1])
    dense_v[...] = branch * dot(dense_hidden, dout_all[...].reshape(units, half))

    for i in range(chunks):
        for d in order:
            place, _ = cross_peer(d)
            arrived(RS + i, r_recv.at[i, place], place)
        part = dot(mix_w[...], r_recv[i].reshape(every, piece))
        part += dense_v[:, i * piece : (i + 1) * piece]
        s_send[i] = part.astype(bf16).reshape(side, rows, piece)
        for d in order:
            place, device = line_peer(d)
            go(to_peer(SS + i, s_send.at[i, place], s_recv.at[i, p], place, device))
        s_recv[i, p] = s_send[i, p]

    shared_copy.wait_recv()
    shared = (shared_own.astype(f32) + sh_recv[...].astype(f32)).astype(bf16).astype(f32)
    skip = residual_alpha * own.astype(f32) + shared
    totals = []
    for i in range(chunks):
        for d in order:
            place, _ = line_peer(d)
            arrived(SS + i, s_recv.at[i, place], place)
        total = skip[:, i * piece : (i + 1) * piece]
        for j in range(side):
            total += s_recv[i, j].astype(f32)
        totals.append(total)
    loaded("fgain", "fshift")
    row_sum = sum(jnp.sum(t, axis=1, keepdims=True) for t in totals)
    row_squares = sum(jnp.sum(t * t, axis=1, keepdims=True) for t in totals)
    st_send[...] = jnp.where(iota(st_send.shape, 1) < 0.5, row_sum, row_squares)
    st_copy = go(to_partner(3, st_send, st_recv))
    st_copy.wait_recv()
    mean = (row_sum + st_recv[:, 0:1]) / width
    variance = (row_squares + st_recv[:, 1:2]) / width - mean * mean
    scale = lax.rsqrt(variance + norm_eps)
    for i in range(chunks):
        at = slice(i * piece, (i + 1) * piece)
        out_ref[:, at] = ((totals[i] - mean) * scale * local["fgain"][:, at] + local["fshift"][:, at]).astype(
            bf16
        )
    for copy in sends:
        copy.wait_send()


def layer(side, cap, experts, args):
    names = tuple(args)
    rows, width = args["x"].shape
    groups, states = args["rate"].shape
    channels = args["win"].shape[1]
    half = width // 2
    chunks = CHUNKS
    piece = half // chunks
    slots = side * cap
    every = side * slots
    lanes = -(-experts // 128) * 128
    din, dout = args["din"], args["dout"]
    kinds = 4 + 4 * chunks
    V = pltpu.VMEM
    return pl.pallas_call(
        functools.partial(layer_kernel, side, cap, names),
        out_shape=(
            jax.ShapeDtypeStruct((rows, half), bf16),
            jax.ShapeDtypeStruct(args["state"].shape, f32),
        ),
        in_specs=[pl.BlockSpec(memory_space=pl.ANY)] * len(names),
        out_specs=(pl.BlockSpec(memory_space=pltpu.VMEM),) * 2,
        scratch_shapes=[V(a.shape, a.dtype) for a in args.values()]
        + [
            V((2, channels, groups * 2 * states), bf16),
            V((2, channels, groups * 2 * states), bf16),
            V((rows, channels), bf16),
            V((2, rows, channels), bf16),
            V((side, 2, rows, lanes), bf16),
            V((side, *din.shape), bf16),
            V((side, *dout.shape), bf16),
            V((chunks, side, rows, piece), bf16),
            V((side, rows, half), bf16),
            V((chunks, side, slots, piece), bf16),
            V((chunks, side, slots, piece), bf16),
            V((chunks, side, slots, piece), bf16),
            V((every, half), bf16),
            V((every, half), bf16),
            V((chunks, side, slots, piece), bf16),
            V((chunks, side, slots, piece), bf16),
            V((chunks, side, rows, piece), bf16),
            V((chunks, side, rows, piece), bf16),
            V((rows, half), bf16),
            V((rows, half), bf16),
            V((rows, 128), f32),
            V((rows, 128), f32),
            V((every, side * rows), bf16),
            V((side * rows, every), bf16),
            V((side * rows, half), f32),
            pltpu.SemaphoreType.DMA((len(names),)),
            pltpu.SemaphoreType.DMA((kinds, side)),
            pltpu.SemaphoreType.DMA((kinds, side)),
            pltpu.SemaphoreType.DMA((4 + chunks,)),
            pltpu.SemaphoreType.DMA((4 + chunks,)),
        ],
        compiler_params=pltpu.CompilerParams(
            collective_id=0, has_side_effects=True, vmem_limit_bytes=VMEM_BYTES
        ),
        name="layer",
    )(*args.values())


def body(
    layer_input,
    ssm_state,
    w_input,
    decay_rate,
    frequency,
    step_log,
    input_map,
    output_map,
    skip_gain,
    glu_weight,
    mix_out,
    norm_gain,
    norm_shift,
    route_ids,
    route_weights,
    gate_expert,
    up_expert,
    down_expert,
    gate_shared,
    up_shared,
    down_shared,
    dense_in,
    dense_out,
    branch_gate,
    final_gain,
    final_shift,
):
    count_ep = lax.axis_size("ep")
    count_tp = lax.axis_size("tp")
    seq_rows, width = layer_input.shape
    top_k = route_ids.shape[1]
    experts = gate_expert.shape[0] * count_ep
    cap = count_tp * max(1, min(seq_rows // count_tp, seq_rows * top_k // experts))
    side = math.isqrt(count_ep)
    layer_output, new_state = layer(
        side,
        cap,
        experts,
        dict(
            ids=route_ids.T,
            scores=route_weights.T,
            rate=decay_rate,
            freq=frequency,
            step=step_log[None],
            imap=input_map.transpose(0, 1, 3, 2),
            omap=output_map,
            skip=skip_gain,
            x=layer_input,
            win=w_input,
            state=ssm_state.reshape(-1, ssm_state.shape[3]),
            din=dense_in,
            dout=dense_out,
            glu=glu_weight,
            mix=mix_out,
            gain=norm_gain[None],
            shift=norm_shift[None],
            gs=gate_shared,
            us=up_shared,
            ds=down_shared,
            ge=gate_expert[0],
            ue=up_expert[0],
            de=down_expert[0],
            bgate=branch_gate[None],
            fgain=final_gain[None],
            fshift=final_shift[None],
        ),
    )
    new_state = new_state.reshape(ssm_state.shape)
    return (layer_output, new_state)


def solution(mesh):
    placed = (
        P(("grp", "ep"), None),
        P(None, ("grp", "ep"), "tp", None),
        P(None, "tp"),
        P("tp", None),
        P("tp", None),
        P("tp"),
        P(None, "tp", None, None),
        P(None, "tp", None, None),
        P("tp", None),
        P(),
        P(),
        P(),
        P(),
        P(("grp", "ep"), None),
        P(("grp", "ep"), None),
        P("ep", None, "tp"),
        P("ep", None, "tp"),
        P("ep", "tp", None),
        P(None, "tp"),
        P(None, "tp"),
        P("tp", None),
        P("ep", None),
        P("ep", "tp"),
        P(),
        P("tp"),
        P("tp"),
    )
    return jax.shard_map(
        body,
        mesh=mesh,
        in_specs=placed,
        out_specs=(P(("grp", "ep"), "tp"), P(None, ("grp", "ep"), "tp", None)),
        check_vma=False,
    )
```

time: 103 us -> 87.3 us (0.85)
  matrix products: 7.22 us -> 0 us
  local copies, waits for them, and re-layouts: 11.1 us -> 4.63 us
    dot_general x5 -> x0, matrix products: 7.22 us -> none  [the longest x1 1.72 us: state_update(): pushed_im = jnp.einsum('gpm,tgm->tgp', drive_im, inputs, precision=highest)]
    unnamed x50 -> x2, local copies, waits for them, and re-layouts: 7.42 us -> 3.34 us
    slice x1 -> x0, local copies, waits for them, and re-layouts: 1.86 us -> none  [state_update(): new_re = decay_re * ssm_state[0] - decay_im * ssm_state[1] + pushed_re]
    broadcast_in_dim x1, local copies, waits for them, and re-layouts: 0.01 us -> 1.29 us  [body(): branch_gate[None]]
where the time goes in v2:
time: 87.3 us; the launch traced here: 87.1 us
  Pallas kernels  81.8 us (94%)
  local copies, waits for them, and re-layouts  4.63 us (5%)
    pallas_call x1, Pallas kernels, layer(): pl.pallas_call(functools.partial(layer_kernel, side, cap, names), out_sha...  81.8 us
    unnamed x2, local copies, waits for them, and re-layouts  3.34 us

profile of v2, /device:TPU:515, one launch (start us, length us, event | category | flops | bytes accessed | tf_op | source)
XLA Modules:
  0.0 87.1 jit_solution(16579598244974682649)
XLA Ops:
  0.6 1.3 %broadcast_in_dim.21.refs_23_ = bf16[1,2048]{1,0:T(2,128)(2,1)} reshape(bf16[2048]{0:T(1024)(128)(2,1)} %param.49) | data formatting | bytes 8192 | tf_op jit(solution)/shard_map/broadcast_in_dim | solution.py:571
  1.9 81.8 %layer.1 = (bf16[32,1024]{1,0:T(8,128)(2,1)}, f32[1024,64]{1,0:T(8,128)}) custom-call(s32[6,32]{1,0:T(8,128)} %bitcast.21, f32[6,32]{1,0:T(8,128)} %bitcast.22, f32[16,64]{1,0:T(8,128)} %refs_2_.1, f32[16,64]{1,0:T(8,128)} %refs_3_.1, f32[1,16]{1,0:T(1,128)} %bitcast.25, f32[2,16,16,64]{3,2,1,0:T(8,128)} %bitcast.18, f32[2,16,16,64]{3,2,1,0:T(8,128)} %refs_6_.1, ...), custom_call_target="tpu_custom_call" | custom-call | tf_op jit(solution)/shard_map/layer/pallas_call | solution.py:460
  83.7 1.5 %copy.30 = bf16[32,1024]{1,0:T(8,128)(2,1)} copy(bf16[32,1024]{1,0:T(8,128)(2,1)} %get-tuple-element.8) | data formatting | bytes 131072
  85.2 1.9 %copy.31 = f32[2,32,16,64]{3,2,1,0:T(8,128)} copy(f32[2,32,16,64]{3,2,1,0:T(8,128)} %bitcast.17) | data formatting | bytes 524288

commit v3 on v2

--- a/solution.py
+++ b/solution.py
@@ -36,18 +36,19 @@
     return high, (a - high.astype(f32)).astype(bf16)
 
 
-def layer_kernel(side, cap, names, *refs):
+def layer_kernel(side, cap, experts, names, *refs):
     count = len(names)
     hbm = refs[:count]
     out_ref, new_ref = refs[count : count + 2]
     local = dict(zip(names, refs[count + 2 :]))
     rest = refs[2 * count + 2 :]
-    layer_steps(side, cap, names, hbm, local, out_ref, new_ref, *rest)
+    layer_steps(side, cap, experts, names, hbm, local, out_ref, new_ref, *rest)
 
 
 def layer_steps(
     side,
     cap,
+    experts,
     names,
     hbm,
     local,
@@ -102,21 +103,24 @@
         return (1 - core) * (qq * side + pp) + core * (pp * side + qq)
 
     def line_peer(d):
-        pp = lax.rem(p + d, side)
+        pp = lax.rem(p + d + side, side)
         return pp, {"ep": chip_at(pp, q), "tp": core}
 
     def cross_peer(d):
-        qq = lax.rem(q + d, side)
+        qq = lax.rem(q + d + side, side)
         return qq, {"ep": chip_at(p, qq), "tp": core}
 
     partner = {"ep": chip, "tp": 1 - core}
+    tree = side == 8
+    near = [d for d in (2, -2, 1, -1) if tree] or list(range(1, side))
     order = sorted(range(1, side), key=lambda d: -min(d, side - d))
 
     META, DIN, DOUT, OTH, OWN = 0, 1, 2, 3, 4
     XS, RS, SS = OWN + chunks, OWN + 2 * chunks, OWN + 3 * chunks
 
-    def to_peer(kind, src, dst, place, device):
-        me = q if kind in (DIN, DOUT) or XS <= kind < SS else p
+    def to_peer(kind, src, dst, place, device, me=None):
+        if me is None:
+            me = q if kind in (DIN, DOUT) or XS <= kind < SS else p
         return pltpu.make_async_remote_copy(
             src_ref=src,
             dst_ref=dst,
@@ -146,6 +150,36 @@
             device_id_type=MESH,
         )
 
+    def spread_out(kind, peer, me, src, dst):
+        for d in near:
+            place, device = peer(d)
+            go(to_peer(kind, src, dst.at[me], place, device))
+
+    def forward(kind, peer, me, dst):
+        if not tree:
+            return
+        way = 1 - 2 * lax.rem(me, 2)
+        for back, on, slot in ((-2, 1, 3), (2, -1, -3)):
+            origin, _ = peer(back)
+            arrived(kind, dst.at[origin], origin)
+            _, device = peer(on)
+            go(to_peer(kind, dst.at[origin], dst.at[origin], peer(slot)[0], device, origin))
+        origin, _ = peer(-2 * way)
+        _, device = peer(2 * way)
+        go(to_peer(kind, dst.at[origin], dst.at[origin], peer(4)[0], device, origin))
+
+    def rest_arrived(kind, peer, dst):
+        for d in (1, -1, 3, -3, 4) if tree else near:
+            place, _ = peer(d)
+            arrived(kind, dst.at[place], place)
+
+    sends = []
+
+    def go(copy):
+        copy.start()
+        sends.append(copy)
+        return copy
+
     loads = {
         name: pltpu.make_async_copy(src, local[name], load_sem.at[i])
         for i, (name, src) in enumerate(zip(names, hbm))
@@ -163,7 +197,7 @@
         for _, device in (line_peer(d), cross_peer(d)):
             pl.semaphore_signal(barrier, inc=1, device_id=device, device_id_type=MESH)
 
-    lanes = meta.shape[3]
+    lanes = meta.shape[2]
     loaded("ids", "scores")
     ids, scores = local["ids"][...].astype(f32), local["scores"][...]
     scores = scores / jnp.sum(scores, axis=0, keepdims=True) * route_scale
@@ -174,13 +208,12 @@
     for k in range(ids.shape[0]):
         name = jnp.sum(jnp.where(eye, ids[k : k + 1], 0.0), axis=1, keepdims=True)
         score = jnp.sum(jnp.where(eye, scores[k : k + 1], 0.0), axis=1, keepdims=True)
-        here = jnp.where(lane == name, 1.0, 0.0)
-        hits += here
-        share += here * score
+        hits += jnp.where(lane == name, 1.0, 0.0)
+        share += jnp.where(lane == name + experts, score, 0.0)
     earlier = jnp.where(iota((rows, rows), 1) < iota((rows, rows), 0), 1.0, 0.0)
     ranks = dot(earlier.astype(bf16), hits.astype(bf16))
-    meta[p, 0] = jnp.where(hits > 0.5, ranks, -1.0).astype(bf16)
-    meta[p, 1] = share.astype(bf16)
+    codes = jnp.where(hits > 0.5, ranks, -1.0)
+    meta[p] = jnp.where(lane < experts, codes, share).astype(bf16)
 
     groups, states = local["rate"].shape
     members = local["skip"].shape[1]
@@ -247,13 +280,6 @@
     act_send[...] = jax.nn.gelu(response).astype(bf16)
 
     pl.semaphore_wait(barrier, 2 * side - 1)
-    sends = []
-
-    def go(copy):
-        copy.start()
-        sends.append(copy)
-        return copy
-
     act_copy = go(to_partner(0, act_send, act_all.at[core]))
     act_all[core] = act_send[...]
     loaded("din", "dout")
@@ -262,10 +288,8 @@
     for d in order:
         place, device = line_peer(d)
         go(to_peer(META, meta.at[p], meta.at[p], place, device))
-    for d in order:
-        place, device = cross_peer(d)
-        go(to_peer(DIN, din_ref, din_all.at[q], place, device))
-        go(to_peer(DOUT, dout_ref, dout_all.at[q], place, device))
+    spread_out(DIN, cross_peer, q, din_ref, din_all)
+    spread_out(DOUT, cross_peer, q, dout_ref, dout_all)
 
     loaded("glu", "mix", "gain", "shift")
     glu_v, mix_v = local["glu"], local["mix"]
@@ -290,9 +314,7 @@
         own_all[i, p] = own[:, i * piece : (i + 1) * piece]
     oth_all[p] = oth
     for i in range(chunks):
-        for d in order:
-            place, device = line_peer(d)
-            go(to_peer(OWN + i, own_all.at[i, p], own_all.at[i, p], place, device))
+        spread_out(OWN + i, line_peer, p, own_all.at[i, p], own_all.at[i])
 
     for d in order:
         place, _ = line_peer(d)
@@ -303,13 +325,16 @@
     at_rank = lane - at_q * slots - at_p * cap
     pf, cf = p.astype(f32), core.astype(f32)
     expert = (1.0 - cf) * (at_q * side + pf) + cf * (pf * side + at_q)
-    spread = jnp.where(iota((lanes, every), 0) == expert, 1.0, 0.0).astype(bf16)
-    codes = dot(meta[:, 0].reshape(line_rows, lanes), spread)
-    shares = dot(meta[:, 1].reshape(line_rows, lanes), spread)
+    at_lane = iota((lanes, every), 0)
+    every_meta = meta[...].reshape(line_rows, lanes)
+    codes = dot(every_meta, jnp.where(at_lane == expert, 1.0, 0.0).astype(bf16))
+    shares = dot(every_meta, jnp.where(at_lane == expert + experts, 1.0, 0.0).astype(bf16))
     block = jnp.floor((iota((line_rows, 1), 0) + 0.5) / rows)
     chosen = jnp.where((codes == at_rank) & (block == at_p), 1.0, 0.0)
     mix_w[...] = (chosen * shares).astype(bf16)
     pick_v[...] = chosen.T.astype(bf16)
+
+    forward(OWN, line_peer, p, own_all.at[0])
 
     loaded("gs", "us", "ds")
     gs_v, us_v, ds_v = local["gs"], local["us"], local["ds"]
@@ -320,10 +345,11 @@
     shared_copy = go(to_partner(1, sh_send, sh_recv))
     shared_own = dot(hidden, ds_v[:, pl.ds(pl.multiple_of(base, 128), half)]).astype(bf16)
 
-    for i in range(chunks):
-        for d in order:
-            place, _ = line_peer(d)
-            arrived(OWN + i, own_all.at[i, place], place)
+    for i in range(1, chunks):
+        forward(OWN + i, line_peer, p, own_all.at[i])
+
+    for i in range(chunks):
+        rest_arrived(OWN + i, line_peer, own_all.at[i])
         picked = dot(pick_v[...], own_all[i].reshape(line_rows, piece)).astype(bf16)
         x_send[i] = picked.reshape(side, slots, piece)
         for d in order:
@@ -341,9 +367,9 @@
             place, _ = cross_peer(d)
             arrived(XS + i, x_recv.at[i, place], place)
         go(to_partner(4 + i, x_recv.at[i], x_oth.at[i]))
-    for d in order:
-        place, device = line_peer(d)
-        go(to_peer(OTH, oth_all.at[p], oth_all.at[p], place, device))
+    forward(DIN, cross_peer, q, din_all)
+    forward(DOUT, cross_peer, q, dout_all)
+    spread_out(OTH, line_peer, p, oth_all.at[p], oth_all)
     loaded("ge", "ue", "de")
     ge_v, ue_v, de_v = local["ge"], local["ue"], local["de"]
     units = ge_v.shape[1]
@@ -364,6 +390,7 @@
     y_send[...] = dot(hidden, de_v[:, pl.ds(pl.multiple_of(other, 128), half)]).astype(bf16)
     y_copy = go(to_partner(2, y_send, y_oth))
     result = dot(hidden, de_v[:, pl.ds(pl.multiple_of(base, 128), half)])
+    forward(OTH, line_peer, p, oth_all)
     y_copy.wait_recv()
     for i in range(chunks):
         at = slice(i * piece, (i + 1) * piece)
@@ -374,20 +401,18 @@
             go(to_peer(RS + i, r_send.at[i, place], r_recv.at[i, q], place, device))
         r_recv[i, q] = r_send[i, q]
 
-    for d in order:
-        place, _ = line_peer(d)
-        arrived(OTH, oth_all.at[place], place)
-    for d in order:
-        place, _ = cross_peer(d)
-        arrived(DIN, din_all.at[place], place)
-        arrived(DOUT, dout_all.at[place], place)
+    rest_arrived(OTH, line_peer, oth_all)
+    rest_arrived(DIN, cross_peer, din_all)
+    rest_arrived(DOUT, cross_peer, dout_all)
     units = side * din_ref.shape[0]
     din = din_all[...].reshape(units, width)
     din_left, din_right = din[:, :half], din[:, half:]
     din_own = jnp.where(first, din_left, din_right)
     din_oth = jnp.where(first, din_right, din_left)
     loaded("bgate")
-    bgate = jnp.broadcast_to(local["bgate"][...], (8, width))
+    bgate = local["bgate"][...].astype(f32)
+    bgate = jnp.concatenate([bgate[k : k + 1] for k in range(bgate.shape[0])], axis=1)
+    bgate = jnp.broadcast_to(bgate, (8, width)).astype(bf16)
     b_own = jnp.where(first, bgate[:, :half], bgate[:, half:])
     b_oth = jnp.where(first, bgate[:, half:], bgate[:, :half])
     oth_tok = oth_all[...].reshape(line_rows, half)
@@ -453,12 +478,12 @@
     piece = half // chunks
     slots = side * cap
     every = side * slots
-    lanes = -(-experts // 128) * 128
+    lanes = -(-2 * experts // 128) * 128
     din, dout = args["din"], args["dout"]
     kinds = 4 + 4 * chunks
     V = pltpu.VMEM
     return pl.pallas_call(
-        functools.partial(layer_kernel, side, cap, names),
+        functools.partial(layer_kernel, side, cap, experts, names),
         out_shape=(
             jax.ShapeDtypeStruct((rows, half), bf16),
             jax.ShapeDtypeStruct(args["state"].shape, f32),
@@ -471,7 +496,7 @@
             V((2, channels, groups * 2 * states), bf16),
             V((rows, channels), bf16),
             V((2, rows, channels), bf16),
-            V((side, 2, rows, lanes), bf16),
+            V((side, rows, lanes), bf16),
             V((side, *din.shape), bf16),
             V((side, *dout.shape), bf16),
             V((chunks, side, rows, piece), bf16),
@@ -568,7 +593,7 @@
             ge=gate_expert[0],
             ue=up_expert[0],
             de=down_expert[0],
-            bgate=branch_gate[None],
+            bgate=branch_gate.reshape(-1, 128),
             fgain=final_gain[None],
             fshift=final_shift[None],
         ),

time: 87.3 us -> 78.5 us (0.90)
  the two profiles are of different devices: /device:TPU:515 before, /device:TPU:513 now
where the time goes in v3:
time: 78.5 us; the launch traced here: 78.3 us
  Pallas kernels  74.3 us (95%)
  local copies, waits for them, and re-layouts  3.34 us (4%)
    pallas_call x1, Pallas kernels, layer(): pl.pallas_call(functools.partial(layer_kernel, side, cap, experts, names)...  74.3 us
    unnamed x2, local copies, waits for them, and re-layouts  3.34 us

profile of v3, /device:TPU:513, one launch (start us, length us, event | category | flops | bytes accessed | tf_op | source)
XLA Modules:
  0.0 78.3 jit_solution(4365927714654551534)
XLA Ops:
  0.6 74.3 %layer.1 = (bf16[32,1024]{1,0:T(8,128)(2,1)}, f32[1024,64]{1,0:T(8,128)}) custom-call(s32[6,32]{1,0:T(8,128)} %bitcast.22, f32[6,32]{1,0:T(8,128)} %bitcast.23, f32[16,64]{1,0:T(8,128)} %refs_2_.1, f32[16,64]{1,0:T(8,128)} %refs_3_.1, f32[1,16]{1,0:T(1,128)} %bitcast.27, f32[2,16,16,64]{3,2,1,0:T(8,128)} %bitcast.19, f32[2,16,16,64]{3,2,1,0:T(8,128)} %refs_6_.1, ...), custom_call_target="tpu_custom_call" | custom-call | tf_op jit(solution)/shard_map/layer/pallas_call | solution.py:485
  74.9 1.5 %copy.30 = bf16[32,1024]{1,0:T(8,128)(2,1)} copy(bf16[32,1024]{1,0:T(8,128)(2,1)} %get-tuple-element.8) | data formatting | bytes 131072
  76.4 1.9 %copy.31 = f32[2,32,16,64]{3,2,1,0:T(8,128)} copy(f32[2,32,16,64]{3,2,1,0:T(8,128)} %bitcast.18) | data formatting | bytes 524288

commit v4 on v3

v4 whole, which is shorter than its diff:
```python
import functools
import math

import jax
import jax.numpy as jnp
from jax import lax
from jax.experimental import pallas as pl
from jax.experimental.pallas import tpu as pltpu
from jax.sharding import PartitionSpec as P

residual_alpha = 1.681792830507429
route_scale = 2.5
norm_eps = 1e-05
highest = lax.Precision.HIGHEST
MESH = pl.DeviceIdType.MESH
f32 = jnp.float32
bf16 = jnp.bfloat16
VMEM_BYTES = 64 * 1024 * 1024 - 1024 * 1024


def dot(a, b):
    return jnp.dot(a, b, preferred_element_type=f32)


def dot_t(a, b):
    return lax.dot_general(a, b, (((1,), (1,)), ((), ())), preferred_element_type=f32)


def iota(shape, dim):
    return lax.broadcasted_iota(jnp.int32, shape, dim).astype(f32)


def halves(a):
    high = a.astype(bf16)
    return high, (a - high.astype(f32)).astype(bf16)


def layer_kernel(side, cap, experts, names, *refs):
    count = len(names)
    hbm = refs[:count]
    out_ref, new_ref = refs[count : count + 2]
    local = dict(zip(names, refs[count + 2 :]))
    rest = refs[2 * count + 2 :]
    layer_steps(side, cap, experts, names, hbm, local, out_ref, new_ref, *rest)


def layer_steps(
    side,
    cap,
    experts,
    names,
    hbm,
    local,
    out_ref,
    new_ref,
    drive_v,
    omap_v,
    act_send,
    act_all,
    meta,
    din_all,
    dout_all,
    own_all,
    oth_all,
    x_send,
    x_recv,
    x_oth,
    y_send,
    y_oth,
    r_send,
    r_recv,
    s_send,
    s_recv,
    relay,
    merged,
    sh_send,
    sh_recv,
    st_send,
    st_recv,
    pick_v,
    mix_w,
    dense_v,
    load_sem,
    send_sem,
    recv_sem,
    tsend_sem,
    trecv_sem,
):
    x_ref, din_ref, dout_ref = local["x"], local["din"], local["dout"]
    rows, width = x_ref.shape
    half = width // 2
    line_rows = side * rows
    group = side // 2
    slots = group * cap
    part_rows = side * slots
    every = 2 * part_rows
    core = lax.axis_index("tp")
    chip = lax.axis_index("ep")
    row, col = lax.div(chip, side), lax.rem(chip, side)
    p = (1 - core) * col + core * row
    q = (1 - core) * row + core * col

    def chip_at(pp, qq):
        return (1 - core) * (qq * side + pp) + core * (pp * side + qq)

    def slot(d):
        d = (d + side - 1) % side
        d = d + 1 - side if d + 1 > side // 2 else d + 1
        return 2 * d - 1 if d > 0 else -2 * d

    def line_peer(d):
        return {"ep": chip_at(lax.rem(p + d + side, side), q), "tp": core}

    def cross_peer(d):
        return {"ep": chip_at(p, lax.rem(q + d + side, side)), "tp": core}

    partner = {"ep": chip, "tp": 1 - core}
    tree = side == 8
    near = [d for d in (2, -2, 1, -1) if tree] or list(range(1, side))
    order = sorted(range(1, side), key=lambda d: -min(d, side - d))
    if tree:
        order = [4, 3, -3, 2, -2, 1, -1]

    META, DIN, DOUT, OTH, OWN, XS, RS, SS = 0, 1, 2, 3, 4, 5, 7, 9

    def send(kind, device, src, dst, sent, landed):
        go(
            pltpu.make_async_remote_copy(
                src_ref=src,
                dst_ref=dst,
                send_sem=send_sem.at[kind, sent],
                recv_sem=recv_sem.at[kind, landed],
                device_id=device,
                device_id_type=MESH,
            )
        )

    def arrived(kind, dst, landed):
        pltpu.make_async_remote_copy(
            src_ref=dst,
            dst_ref=dst,
            send_sem=send_sem.at[kind, landed],
            recv_sem=recv_sem.at[kind, landed],
            device_id=partner,
            device_id_type=MESH,
        ).wait_recv()

    def to_partner(kind, src, dst):
        return pltpu.make_async_remote_copy(
            src_ref=src,
            dst_ref=dst,
            send_sem=tsend_sem.at[kind],
            recv_sem=trecv_sem.at[kind],
            device_id=partner,
            device_id_type=MESH,
        )

    def spread_out(kind, peer, dst, offsets):
        for d in offsets:
            send(kind, peer(d), dst.at[0], dst.at[slot(-d)], slot(d), slot(-d))

    def forward(kind, peer, dst, place):
        if not tree:
            return
        for back, on in ((-2, 1), (2, -1)):
            arrived(kind, dst.at[slot(back)], slot(back))
            to = slot(back - on)
            send(kind, peer(on), dst.at[slot(back)], dst.at[to], slot(on - back), to)
        way = 1 - 2 * lax.rem(place, 2)
        middle = lax.div(7 + way, 2)
        send(kind, peer(2 * way), dst.at[middle], dst.at[slot(4)], slot(4), slot(4))

    def rest_arrived(kind, dst, offsets):
        for d in offsets:
            arrived(kind, dst.at[slot(d)], slot(d))

    beyond = [1, -1, 3, -3, 4] if tree else near

    sends = []

    def go(copy):
        copy.start()
        sends.append(copy)
        return copy

    loads = {
        name: pltpu.make_async_copy(src, local[name], load_sem.at[i])
        for i, (name, src) in enumerate(zip(names, hbm))
    }
    later = names.index("din")
    for name in names[:later]:
        loads[name].start()
    barrier = pltpu.get_barrier_semaphore()
    pl.semaphore_signal(barrier, inc=1, device_id=partner, device_id_type=MESH)
    for d in range(1, side):
        for device in (line_peer(d), cross_peer(d)):
            pl.semaphore_signal(barrier, inc=1, device_id=device, device_id_type=MESH)
    for name in names[later:]:
        loads[name].start()

    def loaded(*wanted):
        for name in wanted:
            loads[name].wait()

    groups, states = local["rate"].shape
    members = local["skip"].shape[1]
    channels = groups * members
    pair = 2 * states
    drive_v[...] = jnp.zeros_like(drive_v)
    omap_v[...] = jnp.zeros_like(omap_v)
    loaded("rate", "freq", "step", "imap", "omap", "skip")
    rate, freq = local["rate"][...], local["freq"][...]
    eye = iota((groups, groups), 0) == iota((groups, groups), 1)
    step = jnp.exp(jnp.sum(jnp.where(eye, local["step"][...], 0.0), axis=1, keepdims=True))
    magnitude = jnp.exp(-rate * step)
    angle = freq * step
    decay_re, decay_im = magnitude * jnp.cos(angle), magnitude * jnp.sin(angle)
    denominator = rate * rate + freq * freq
    factor_re = ((decay_re - 1.0) * -rate + decay_im * freq) / denominator
    factor_im = (decay_im * -rate - (decay_re - 1.0) * freq) / denominator
    same = jnp.concatenate([decay_re, decay_re], axis=1)
    cross = jnp.concatenate([-decay_im, decay_im], axis=1)
    for g in range(groups):
        fr, fi = factor_re[g : g + 1], factor_im[g : g + 1]
        m0, m1 = local["imap"][0, g], local["imap"][1, g]
        drive = jnp.concatenate([fr * m0 - fi * m1, fr * m1 + fi * m0], axis=1)
        out = jnp.concatenate([local["omap"][0, g], -local["omap"][1, g]], axis=1)
        at, lanes_at = slice(g * members, (g + 1) * members), slice(g * pair, (g + 1) * pair)
        drive_v[0, at, lanes_at], drive_v[1, at, lanes_at] = halves(drive)
        omap_v[at, lanes_at] = out.astype(bf16)
    tile = jnp.where(
        iota((members, channels), 0)
        == iota((members, channels), 1)
        - jnp.floor((iota((members, channels), 1) + 0.5) / members) * members,
        1.0,
        0.0,
    )
    skip = jnp.dot(local["skip"][...], tile, preferred_element_type=f32, precision=highest)
    in_group = jnp.floor((iota((groups, channels), 1) + 0.5) / members) == iota(
        (groups, channels), 0
    )
    skip = jnp.sum(jnp.where(in_group, skip, 0.0), axis=0, keepdims=True)
    loaded("x", "win")
    projected = dot(x_ref[...], local["win"][...]).astype(bf16)
    pushed = dot(projected, drive_v[0]) + dot(projected, drive_v[1])
    loaded("state")
    response = skip * projected.astype(f32)
    states_now = []
    for g in range(groups):
        old = jnp.concatenate(
            [
                local["state"][pl.ds(g, rows, stride=groups)],
                local["state"][pl.ds(rows * groups + g, rows, stride=groups)],
            ],
            axis=1,
        )
        turned = jnp.concatenate([old[:, states:], old[:, :states]], axis=1)
        new = same[g : g + 1] * old + cross[g : g + 1] * turned
        new += pushed[:, g * pair : (g + 1) * pair]
        new_ref[pl.ds(g, rows, stride=groups)] = new[:, :states]
        new_ref[pl.ds(rows * groups + g, rows, stride=groups)] = new[:, states:]
        states_now.append(new.astype(bf16))
    response += dot_t(jnp.concatenate(states_now, axis=1), omap_v[...])
    act_send[...] = jax.nn.gelu(response).astype(bf16)

    pl.semaphore_wait(barrier, 2 * side - 1)
    act_copy = go(to_partner(0, act_send, act_all.at[core]))
    act_all[core] = act_send[...]
    loaded("din", "dout")
    din_all[0] = din_ref[...]
    dout_all[0] = dout_ref[...]
    spread_out(DIN, cross_peer, din_all, near)
    spread_out(DOUT, cross_peer, dout_all, near)

    lanes = meta.shape[2]
    loaded("ids", "scores")
    ids, scores = local["ids"][...].astype(f32), local["scores"][...]
    scores = scores / jnp.sum(scores, axis=0, keepdims=True) * route_scale
    eye = iota((rows, rows), 0) == iota((rows, rows), 1)
    lane = iota((rows, lanes), 1)
    hits = jnp.zeros((rows, lanes), f32)
    share = jnp.zeros((rows, lanes), f32)
    for k in range(ids.shape[0]):
        name = jnp.sum(jnp.where(eye, ids[k : k + 1], 0.0), axis=1, keepdims=True)
        score = jnp.sum(jnp.where(eye, scores[k : k + 1], 0.0), axis=1, keepdims=True)
        hits += jnp.where(lane == name, 1.0, 0.0)
        share += jnp.where(lane == name + experts, score, 0.0)
    earlier = jnp.where(iota((rows, rows), 1) < iota((rows, rows), 0), 1.0, 0.0)
    ranks = dot(earlier.astype(bf16), hits.astype(bf16))
    codes = jnp.where(hits > 0.5, ranks, -1.0)
    meta[0] = jnp.where(lane < experts, codes, share).astype(bf16)
    spread_out(META, line_peer, meta, order)

    loaded("glu", "mix", "gain", "shift")
    glu_v, mix_v = local["glu"], local["mix"]
    act_copy.wait_recv()
    a0, a1 = act_all[0], act_all[1]
    gate = dot(a0, glu_v[:channels]) + dot(a1, glu_v[channels:])
    g0 = (a0.astype(f32) * jax.nn.sigmoid(gate[:, :channels])).astype(bf16)
    g1 = (a1.astype(f32) * jax.nn.sigmoid(gate[:, channels:])).astype(bf16)
    mixed = (dot(g0, mix_v[:channels]) + dot(g1, mix_v[channels:])).astype(bf16)
    values = residual_alpha * x_ref[...].astype(f32) + mixed.astype(f32)
    mean = jnp.mean(values, axis=1, keepdims=True)
    centred = values - mean
    variance = jnp.mean(centred * centred, axis=1, keepdims=True)
    normed = (centred * lax.rsqrt(variance + norm_eps) * local["gain"][...] + local["shift"][...]).astype(
        bf16
    )
    left, right = normed[:, :half], normed[:, half:]
    first = core == 0
    own = jnp.where(first, left, right)
    oth = jnp.where(first, right, left)
    own_all[0] = own
    oth_all[0] = oth
    spread_out(OWN, line_peer, own_all, near)

    rest_arrived(META, meta, order)

    def steps(index):
        odd = index - 2.0 * jnp.floor((index + 0.5) / 2.0)
        ahead = jnp.floor((index + 1.5) / 2.0)
        return jnp.where(odd > 0.5, ahead, -ahead)

    def parts_of(index):
        part = jnp.floor((index + 0.5) / part_rows)
        index = index - part * part_rows
        cross_slot = jnp.floor((index + 0.5) / slots)
        index = index - cross_slot * slots
        member = jnp.floor((index + 0.5) / cap)
        return cross_slot, part * group + member, index - member * cap

    cross_slot, line_slot, at_rank = parts_of(iota((1, every), 1))
    pf, qf, cf = p.astype(f32), q.astype(f32), core.astype(f32)
    at_q = qf + steps(cross_slot)
    at_q = at_q - side * jnp.floor((at_q + 0.5) / side)
    expert = (1.0 - cf) * (at_q * side + pf) + cf * (pf * side + at_q)
    at_lane = iota((lanes, every), 0)
    every_meta = meta[...].reshape(line_rows, lanes)
    codes = dot(every_meta, jnp.where(at_lane == expert, 1.0, 0.0).astype(bf16))
    shares = dot(every_meta, jnp.where(at_lane == expert + experts, 1.0, 0.0).astype(bf16))
    block = jnp.floor((iota((line_rows, 1), 0) + 0.5) / rows)
    chosen = jnp.where((codes == at_rank) & (block == line_slot), 1.0, 0.0)
    weighted = (chosen * shares).astype(bf16)
    part_tokens = group * rows
    for h in range(2):
        tokens = slice(h * part_tokens, (h + 1) * part_tokens)
        lanes_at = slice(h * part_rows, (h + 1) * part_rows)
        mix_w[h] = weighted[tokens, lanes_at]
        pick_v[h] = chosen[tokens, lanes_at].T.astype(bf16)

    forward(OWN, line_peer, own_all, p)

    loaded("gs", "us", "ds")
    gs_v, us_v, ds_v = local["gs"], local["us"], local["ds"]
    hidden = (jax.nn.silu(dot(normed, gs_v[...])) * dot(normed, us_v[...])).astype(bf16)
    base = core * half
    other = (1 - core) * half
    sh_send[...] = dot(hidden, ds_v[:, pl.ds(pl.multiple_of(other, 128), half)]).astype(bf16)
    shared_copy = go(to_partner(1, sh_send, sh_recv))
    shared_own = dot(hidden, ds_v[:, pl.ds(pl.multiple_of(base, 128), half)]).astype(bf16)

    for h in range(2):
        first_ones = [1, -1] if h == 0 else [3, -3, 4]
        if not tree:
            first_ones = [d for d in near if slot(d) // group == h]
        rest_arrived(OWN, own_all, first_ones)
        tokens = own_all[h * group : (h + 1) * group].reshape(part_tokens, half)
        x_send[h] = dot(pick_v[h], tokens).astype(bf16).reshape(side, slots, half)
        for d in order:
            place = slot(d)
            send(
                XS + h, cross_peer(d), x_send.at[h, place], x_recv.at[h, slot(-d)], place, slot(-d)
            )
        x_recv[h, 0] = x_send[h, 0]

    mine = parts_of(iota((every, 1), 0))
    theirs = parts_of(iota((1, every), 1))
    swap = jnp.where(
        (mine[0] == theirs[1]) & (mine[1] == theirs[0]) & (mine[2] == theirs[2]), 1.0, 0.0
    ).astype(bf16)

    for h in range(2):
        for d in order:
            arrived(XS + h, x_recv.at[h, slot(d)], slot(d))
        go(to_partner(4 + h, x_recv.at[h], x_oth.at[h]))
    spread_out(OTH, line_peer, oth_all, near)
    forward(DIN, cross_peer, din_all, q)
    forward(DOUT, cross_peer, dout_all, q)
    loaded("ge", "ue", "de")
    ge_v, ue_v, de_v = local["ge"], local["ue"], local["de"]
    tok = x_recv[...].reshape(every, half)
    at = pl.ds(pl.multiple_of(base, 128), half)
    gate, up = dot(tok, ge_v[at]), dot(tok, ue_v[at])
    for h in range(2):
        to_partner(4 + h, x_recv.at[h], x_oth.at[h]).wait_recv()
    tok = dot(swap, x_oth[...].reshape(every, half)).astype(bf16)
    at = pl.ds(pl.multiple_of(other, 128), half)
    gate += dot(tok, ge_v[at])
    up += dot(tok, ue_v[at])
    hidden = (jax.nn.silu(gate) * up).astype(bf16)
    down_own = de_v[:, pl.ds(pl.multiple_of(base, 128), half)]
    down_other = de_v[:, pl.ds(pl.multiple_of(other, 128), half)]
    for_partner = dot(swap, hidden).astype(bf16)
    for h in (1, 0):
        at = slice(h * part_rows, (h + 1) * part_rows)
        y_send[h] = dot(for_partner[at], down_other).astype(bf16)
        go(to_partner(2 if h else 6, y_send.at[h], y_oth.at[h]))
    result = dot(hidden, down_own)
    for h in (1, 0):
        to_partner(2 if h else 6, y_send.at[h], y_oth.at[h]).wait_recv()
        at = slice(h * part_rows, (h + 1) * part_rows)
        total = result[at] + y_oth[h].astype(f32)
        r_send[h] = total.astype(bf16).reshape(side, slots, half)
        for d in order:
            place = slot(d)
            send(
                RS + h, cross_peer(d), r_send.at[h, place], r_recv.at[h, slot(-d)], place, slot(-d)
            )
        r_recv[h, 0] = r_send[h, 0]
        if h:
            forward(OTH, line_peer, oth_all, p)

    rest_arrived(OTH, oth_all, beyond)
    rest_arrived(DIN, din_all, beyond)
    rest_arrived(DOUT, dout_all, beyond)
    units = side * din_ref.shape[0]
    din = din_all[...].reshape(units, width)
    din_left, din_right = din[:, :half], din[:, half:]
    din_own = jnp.where(first, din_left, din_right)
    din_oth = jnp.where(first, din_right, din_left)
    loaded("bgate")
    bgate = local["bgate"][...].astype(f32)
    bgate = jnp.concatenate([bgate[k : k + 1] for k in range(bgate.shape[0])], axis=1)
    bgate = jnp.broadcast_to(bgate, (8, width)).astype(bf16)
    b_own = jnp.where(first, bgate[:, :half], bgate[:, half:])
    b_oth = jnp.where(first, bgate[:, half:], bgate[:, :half])
    oth_tok = oth_all[...].reshape(line_rows, half)
    own_tok = own_all[...].reshape(line_rows, half)
    before = dot_t(oth_tok, din_oth) + dot_t(own_tok, din_own)
    gate = dot_t(oth_tok, b_oth) + dot_t(own_tok, b_own)
    dense_hidden = jax.nn.gelu(before).astype(bf16)
    branch = jax.nn.sigmoid(gate[:, :1])
    dense_v[...] = branch * dot(dense_hidden, dout_all[...].reshape(units, half))

    def send_sum(on, src, dst, sent, landed):
        send(SS, line_peer(on), src, dst, sent, landed)

    way = 1 - 2 * lax.rem(p, 2)
    for h in (1, 0):
        for d in order:
            arrived(RS + h, r_recv.at[h, slot(d)], slot(d))
        tokens = slice(h * part_tokens, (h + 1) * part_tokens)
        part = dot(mix_w[h], r_recv[h].reshape(part_rows, half)) + dense_v[tokens]
        s_send[h * group : (h + 1) * group] = part.astype(bf16).reshape(group, rows, half)
        if not tree:
            for d in order:
                if slot(d) // group == h:
                    send_sum(d, s_send.at[slot(d)], s_recv.at[slot(-d)], slot(d), slot(-d))
        elif h:
            send_sum(-2 * way, s_send.at[slot(4)], relay.at[2], slot(4), slot(4))
            send_sum(-1, s_send.at[slot(-3)], relay.at[0], slot(-3), slot(3))
            send_sum(1, s_send.at[slot(3)], relay.at[1], slot(3), slot(-3))
        else:
            for d in (1, -1):
                send_sum(d, s_send.at[slot(d)], s_recv.at[slot(-d)], slot(d), slot(-d))
    if tree:
        for k, d in enumerate((3, -3, 4)):
            arrived(SS, relay.at[k], slot(d))
        third = relay[2].astype(f32)
        for k, d in enumerate((-2, 2)):
            mine = s_send[slot(d)].astype(f32) + relay[k].astype(f32)
            mine += jnp.where(d * way < 0, third, 0.0)
            merged[k] = mine.astype(bf16)
            send_sum(d, merged.at[k], s_recv.at[slot(-d)], slot(d), slot(-d))

    shared_copy.wait_recv()
    shared = (shared_own.astype(f32) + sh_recv[...].astype(f32)).astype(bf16).astype(f32)
    skip = residual_alpha * own.astype(f32) + shared
    total = skip + s_send[0].astype(f32)
    for d in near:
        arrived(SS, s_recv.at[slot(d)], slot(d))
        total += s_recv[slot(d)].astype(f32)
    loaded("fgain", "fshift")
    row_sum = jnp.sum(total, axis=1, keepdims=True)
    row_squares = jnp.sum(total * total, axis=1, keepdims=True)
    st_send[...] = jnp.where(iota(st_send.shape, 1) < 0.5, row_sum, row_squares)
    st_copy = go(to_partner(3, st_send, st_recv))
    st_copy.wait_recv()
    mean = (row_sum + st_recv[:, 0:1]) / width
    variance = (row_squares + st_recv[:, 1:2]) / width - mean * mean
    scale = lax.rsqrt(variance + norm_eps)
    out = (total - mean) * scale * local["fgain"][...] + local["fshift"][...]
    out_ref[...] = out.astype(bf16)
    for copy in sends:
        copy.wait_send()


def layer(side, cap, experts, args):
    names = tuple(args)
    rows, width = args["x"].shape
    groups, states = args["rate"].shape
    channels = args["win"].shape[1]
    half = width // 2
    group = side // 2
    slots = group * cap
    part_rows = side * slots
    every = 2 * part_rows
    lanes = -(-2 * experts // 128) * 128
    din, dout = args["din"], args["dout"]
    kinds = 10
    V = pltpu.VMEM
    return pl.pallas_call(
        functools.partial(layer_kernel, side, cap, experts, names),
        out_shape=(
            pltpu.VMEM((rows, half), bf16),
            pltpu.VMEM(args["state"].shape, f32),
        ),
        in_specs=[pl.BlockSpec(memory_space=pl.ANY)] * len(names),
        out_specs=(pl.BlockSpec(memory_space=pltpu.VMEM),) * 2,
        scratch_shapes=[V(a.shape, a.dtype) for a in args.values()]
        + [
            V((2, channels, groups * 2 * states), bf16),
            V((channels, groups * 2 * states), bf16),
            V((rows, channels), bf16),
            V((2, rows, channels), bf16),
            V((side, rows, lanes), bf16),
            V((side, *din.shape), bf16),
            V((side, *dout.shape), bf16),
            V((side, rows, half), bf16),
            V((side, rows, half), bf16),
            V((2, side, slots, half), bf16),
            V((2, side, slots, half), bf16),
            V((2, side, slots, half), bf16),
            V((2, part_rows, half), bf16),
            V((2, part_rows, half), bf16),
            V((2, side, slots, half), bf16),
            V((2, side, slots, half), bf16),
            V((side, rows, half), bf16),
            V((side, rows, half), bf16),
            V((3, rows, half), bf16),
            V((2, rows, half), bf16),
            V((rows, half), bf16),
            V((rows, half), bf16),
            V((rows, 128), f32),
            V((rows, 128), f32),
            V((2, part_rows, group * rows), bf16),
            V((2, group * rows, part_rows), bf16),
            V((side * rows, half), f32),
            pltpu.SemaphoreType.DMA((len(names),)),
            pltpu.SemaphoreType.DMA((kinds, side)),
            pltpu.SemaphoreType.DMA((kinds, side)),
            pltpu.SemaphoreType.DMA((7,)),
            pltpu.SemaphoreType.DMA((7,)),
        ],
        compiler_params=pltpu.CompilerParams(
            collective_id=0, has_side_effects=True, vmem_limit_bytes=VMEM_BYTES
        ),
        name="layer",
    )(*args.values())


def body(
    layer_input,
    ssm_state,
    w_input,
    decay_rate,
    frequency,
    step_log,
    input_map,
    output_map,
    skip_gain,
    glu_weight,
    mix_out,
    norm_gain,
    norm_shift,
    route_ids,
    route_weights,
    gate_expert,
    up_expert,
    down_expert,
    gate_shared,
    up_shared,
    down_shared,
    dense_in,
    dense_out,
    branch_gate,
    final_gain,
    final_shift,
):
    count_ep = lax.axis_size("ep")
    count_tp = lax.axis_size("tp")
    seq_rows, width = layer_input.shape
    top_k = route_ids.shape[1]
    experts = gate_expert.shape[0] * count_ep
    cap = count_tp * max(1, min(seq_rows // count_tp, seq_rows * top_k // experts))
    side = math.isqrt(count_ep)
    layer_output, new_state = layer(
        side,
        cap,
        experts,
        dict(
            ids=route_ids.T,
            scores=route_weights.T,
            rate=decay_rate,
            freq=frequency,
            step=step_log[None],
            imap=input_map.transpose(0, 1, 3, 2),
            omap=output_map,
            skip=skip_gain,
            x=layer_input,
            win=w_input,
            state=ssm_state.reshape(-1, ssm_state.shape[3]),
            din=dense_in,
            dout=dense_out,
            glu=glu_weight,
            mix=mix_out,
            gain=norm_gain[None],
            shift=norm_shift[None],
            gs=gate_shared,
            us=up_shared,
            ds=down_shared,
            ge=gate_expert[0],
            ue=up_expert[0],
            de=down_expert[0],
            bgate=branch_gate.reshape(-1, 128),
            fgain=final_gain[None],
            fshift=final_shift[None],
        ),
    )
    new_state = new_state.reshape(ssm_state.shape)
    return (layer_output, new_state)


def solution(mesh):
    placed = (
        P(("grp", "ep"), None),
        P(None, ("grp", "ep"), "tp", None),
        P(None, "tp"),
        P("tp", None),
        P("tp", None),
        P("tp"),
        P(None, "tp", None, None),
        P(None, "tp", None, None),
        P("tp", None),
        P(),
        P(),
        P(),
        P(),
        P(("grp", "ep"), None),
        P(("grp", "ep"), None),
        P("ep", None, "tp"),
        P("ep", None, "tp"),
        P("ep", "tp", None),
        P(None, "tp"),
        P(None, "tp"),
        P("tp", None),
        P("ep", None),
        P("ep", "tp"),
        P(),
        P("tp"),
        P("tp"),
    )
    return jax.shard_map(
        body,
        mesh=mesh,
        in_specs=placed,
        out_specs=(P(("grp", "ep"), "tp"), P(None, ("grp", "ep"), "tp", None)),
        check_vma=False,
    )
```

time: 78.5 us -> 71.7 us (0.913)
  Pallas kernels: 74.3 us -> 69.6 us
  local copies, waits for them, and re-layouts: 3.34 us -> 1.42 us
    pallas_call x1, Pallas kernels: 74.3 us -> 69.6 us  [layer(): pl.pallas_call(functools.partial(layer_kernel, side, cap, experts, names)...]
    unnamed x2, local copies, waits for them, and re-layouts: 3.34 us -> 1.42 us
where the time goes in v4:
time: 71.7 us; the launch traced here: 71.6 us
  Pallas kernels  69.6 us (97%)
  local copies, waits for them, and re-layouts  1.42 us (2%)
    pallas_call x1, Pallas kernels, layer(): pl.pallas_call(functools.partial(layer_kernel, side, cap, experts, names)...  69.6 us

profile of v4, /device:TPU:513, one launch (start us, length us, event | category | flops | bytes accessed | tf_op | source)
XLA Modules:
  0.0 71.6 jit_solution(489912781352215741)
XLA Ops:
  0.6 69.6 %layer.1 = (bf16[32,1024]{1,0:T(8,128)(2,1)S(1)}, f32[1024,64]{1,0:T(8,128)S(1)}) custom-call(s32[6,32]{1,0:T(8,128)} %bitcast.22, f32[6,32]{1,0:T(8,128)} %bitcast.23, f32[16,64]{1,0:T(8,128)} %refs_2_.1, f32[16,64]{1,0:T(8,128)} %refs_3_.1, f32[1,16]{1,0:T(1,128)} %bitcast.27, f32[2,16,16,64]{3,2,1,0:T(8,128)} %bitcast.19, f32[2,16,16,64]{3,2,1,0:T(8,128)} %refs_6_.1, ...), custom_call_target="tpu_custom_call" | custom-call | tf_op jit(solution)/shard_map/layer/pallas_call | solution.py:512
  70.2 0.6 copy.30
  70.8 0.8 %copy.31 = f32[2,32,16,64]{3,2,1,0:T(8,128)} copy(f32[2,32,16,64]{3,2,1,0:T(8,128)S(1)} %bitcast.14) | data formatting | bytes 524288

commit v5 on v4

--- a/solution.py
+++ b/solution.py
@@ -195,7 +195,8 @@
     for d in range(1, side):
         for device in (line_peer(d), cross_peer(d)):
             pl.semaphore_signal(barrier, inc=1, device_id=device, device_id_type=MESH)
-    for name in names[later:]:
+    bulk = names.index("gs")
+    for name in names[later:bulk]:
         loads[name].start()
 
     def loaded(*wanted):
@@ -225,9 +226,10 @@
         m0, m1 = local["imap"][0, g], local["imap"][1, g]
         drive = jnp.concatenate([fr * m0 - fi * m1, fr * m1 + fi * m0], axis=1)
         out = jnp.concatenate([local["omap"][0, g], -local["omap"][1, g]], axis=1)
-        at, lanes_at = slice(g * members, (g + 1) * members), slice(g * pair, (g + 1) * pair)
-        drive_v[0, at, lanes_at], drive_v[1, at, lanes_at] = halves(drive)
-        omap_v[at, lanes_at] = out.astype(bf16)
+        odd = g % 2
+        at, lanes_at = pl.ds(odd * members, members), pl.ds(odd * pair, pair)
+        drive_v[0, g // 2, at, lanes_at], drive_v[1, g // 2, at, lanes_at] = halves(drive)
+        omap_v[g // 2, at, lanes_at] = out.astype(bf16)
     tile = jnp.where(
         iota((members, channels), 0)
         == iota((members, channels), 1)
@@ -241,8 +243,13 @@
     )
     skip = jnp.sum(jnp.where(in_group, skip, 0.0), axis=0, keepdims=True)
     loaded("x", "win")
+    for name in names[bulk:]:
+        loads[name].start()
     projected = dot(x_ref[...], local["win"][...]).astype(bf16)
-    pushed = dot(projected, drive_v[0]) + dot(projected, drive_v[1])
+    pushed = []
+    for j in range(groups // 2):
+        inputs = projected[:, 2 * j * members : 2 * (j + 1) * members]
+        pushed.append(dot(inputs, drive_v[0, j]) + dot(inputs, drive_v[1, j]))
     loaded("state")
     response = skip * projected.astype(f32)
     states_now = []
@@ -256,11 +263,17 @@
         )
         turned = jnp.concatenate([old[:, states:], old[:, :states]], axis=1)
         new = same[g : g + 1] * old + cross[g : g + 1] * turned
-        new += pushed[:, g * pair : (g + 1) * pair]
+        new += pushed[g // 2][:, g % 2 * pair : (g % 2 + 1) * pair]
         new_ref[pl.ds(g, rows, stride=groups)] = new[:, :states]
         new_ref[pl.ds(rows * groups + g, rows, stride=groups)] = new[:, states:]
         states_now.append(new.astype(bf16))
-    response += dot_t(jnp.concatenate(states_now, axis=1), omap_v[...])
+    response += jnp.concatenate(
+        [
+            dot_t(jnp.concatenate(states_now[2 * j : 2 * j + 2], axis=1), omap_v[j])
+            for j in range(groups // 2)
+        ],
+        axis=1,
+    )
     act_send[...] = jax.nn.gelu(response).astype(bf16)
 
     pl.semaphore_wait(barrier, 2 * side - 1)
@@ -356,7 +369,7 @@
     base = core * half
     other = (1 - core) * half
     sh_send[...] = dot(hidden, ds_v[:, pl.ds(pl.multiple_of(other, 128), half)]).astype(bf16)
-    shared_copy = go(to_partner(1, sh_send, sh_recv))
+    shared_copy = go(to_partner(4 + 2 * side, sh_send, sh_recv))
     shared_own = dot(hidden, ds_v[:, pl.ds(pl.multiple_of(base, 128), half)]).astype(bf16)
 
     for h in range(2):
@@ -379,10 +392,14 @@
         (mine[0] == theirs[1]) & (mine[1] == theirs[0]) & (mine[2] == theirs[2]), 1.0, 0.0
     ).astype(bf16)
 
+    def hand_over(h, k):
+        return to_partner(4 + h * side + k, x_recv.at[h, k], x_oth.at[h, k])
+
     for h in range(2):
+        go(hand_over(h, 0))
         for d in order:
             arrived(XS + h, x_recv.at[h, slot(d)], slot(d))
-        go(to_partner(4 + h, x_recv.at[h], x_oth.at[h]))
+            go(hand_over(h, slot(d)))
     spread_out(OTH, line_peer, oth_all, near)
     forward(DIN, cross_peer, din_all, q)
     forward(DOUT, cross_peer, dout_all, q)
@@ -392,7 +409,8 @@
     at = pl.ds(pl.multiple_of(base, 128), half)
     gate, up = dot(tok, ge_v[at]), dot(tok, ue_v[at])
     for h in range(2):
-        to_partner(4 + h, x_recv.at[h], x_oth.at[h]).wait_recv()
+        for k in range(side):
+            hand_over(h, k).wait_recv()
     tok = dot(swap, x_oth[...].reshape(every, half)).astype(bf16)
     at = pl.ds(pl.multiple_of(other, 128), half)
     gate += dot(tok, ge_v[at])
@@ -404,10 +422,10 @@
     for h in (1, 0):
         at = slice(h * part_rows, (h + 1) * part_rows)
         y_send[h] = dot(for_partner[at], down_other).astype(bf16)
-        go(to_partner(2 if h else 6, y_send.at[h], y_oth.at[h]))
+        go(to_partner(2 if h else 1, y_send.at[h], y_oth.at[h]))
     result = dot(hidden, down_own)
     for h in (1, 0):
-        to_partner(2 if h else 6, y_send.at[h], y_oth.at[h]).wait_recv()
+        to_partner(2 if h else 1, y_send.at[h], y_oth.at[h]).wait_recv()
         at = slice(h * part_rows, (h + 1) * part_rows)
         total = result[at] + y_oth[h].astype(f32)
         r_send[h] = total.astype(bf16).reshape(side, slots, half)
@@ -446,6 +464,14 @@
         send(SS, line_peer(on), src, dst, sent, landed)
 
     way = 1 - 2 * lax.rem(p, 2)
+
+    def merge(k, d):
+        arrived(SS, relay.at[k], slot(3 - 6 * k))
+        mine = s_send[slot(d)].astype(f32) + relay[k].astype(f32)
+        mine += jnp.where(d * way < 0, relay[2].astype(f32), 0.0)
+        merged[k] = mine.astype(bf16)
+        send_sum(d, merged.at[k], s_recv.at[slot(-d)], slot(d), slot(-d))
+
     for h in (1, 0):
         for d in order:
             arrived(RS + h, r_recv.at[h, slot(d)], slot(d))
@@ -460,18 +486,12 @@
             send_sum(-2 * way, s_send.at[slot(4)], relay.at[2], slot(4), slot(4))
             send_sum(-1, s_send.at[slot(-3)], relay.at[0], slot(-3), slot(3))
             send_sum(1, s_send.at[slot(3)], relay.at[1], slot(3), slot(-3))
+            arrived(SS, relay.at[2], slot(4))
+            merge(0, -2)
         else:
+            merge(1, 2)
             for d in (1, -1):
                 send_sum(d, s_send.at[slot(d)], s_recv.at[slot(-d)], slot(d), slot(-d))
-    if tree:
-        for k, d in enumerate((3, -3, 4)):
-            arrived(SS, relay.at[k], slot(d))
-        third = relay[2].astype(f32)
-        for k, d in enumerate((-2, 2)):
-            mine = s_send[slot(d)].astype(f32) + relay[k].astype(f32)
-            mine += jnp.where(d * way < 0, third, 0.0)
-            merged[k] = mine.astype(bf16)
-            send_sum(d, merged.at[k], s_recv.at[slot(-d)], slot(d), slot(-d))
 
     shared_copy.wait_recv()
     shared = (shared_own.astype(f32) + sh_recv[...].astype(f32)).astype(bf16).astype(f32)
@@ -519,8 +539,8 @@
         out_specs=(pl.BlockSpec(memory_space=pltpu.VMEM),) * 2,
         scratch_shapes=[V(a.shape, a.dtype) for a in args.values()]
         + [
-            V((2, channels, groups * 2 * states), bf16),
-            V((channels, groups * 2 * states), bf16),
+            V((2, groups // 2, 2 * channels // groups, 4 * states), bf16),
+            V((groups // 2, 2 * channels // groups, 4 * states), bf16),
             V((rows, channels), bf16),
             V((2, rows, channels), bf16),
             V((side, rows, lanes), bf16),
@@ -549,14 +569,36 @@
             pltpu.SemaphoreType.DMA((len(names),)),
             pltpu.SemaphoreType.DMA((kinds, side)),
             pltpu.SemaphoreType.DMA((kinds, side)),
-            pltpu.SemaphoreType.DMA((7,)),
-            pltpu.SemaphoreType.DMA((7,)),
+            pltpu.SemaphoreType.DMA((5 + 2 * side,)),
+            pltpu.SemaphoreType.DMA((5 + 2 * side,)),
         ],
         compiler_params=pltpu.CompilerParams(
             collective_id=0, has_side_effects=True, vmem_limit_bytes=VMEM_BYTES
         ),
         name="layer",
     )(*args.values())
+
+
+def write_out(*refs):
+    count = (len(refs) - 1) // 2
+    copies = [
+        pltpu.make_async_copy(refs[i], refs[count + i], refs[-1].at[i]) for i in range(count)
+    ]
+    for copy in copies:
+        copy.start()
+    for copy in copies:
+        copy.wait()
+
+
+def to_memory(*arrays):
+    return pl.pallas_call(
+        write_out,
+        out_shape=tuple(jax.ShapeDtypeStruct(a.shape, a.dtype) for a in arrays),
+        in_specs=[pl.BlockSpec(memory_space=pltpu.VMEM)] * len(arrays),
+        out_specs=(pl.BlockSpec(memory_space=pltpu.HBM),) * len(arrays),
+        scratch_shapes=[pltpu.SemaphoreType.DMA((len(arrays),))],
+        name="write_out",
+    )(*(pltpu.with_memory_space_constraint(a, pltpu.VMEM) for a in arrays))
 
 
 def body(
@@ -627,6 +669,7 @@
             fshift=final_shift[None],
         ),
     )
+    layer_output, new_state = to_memory(layer_output, new_state)
     new_state = new_state.reshape(ssm_state.shape)
     return (layer_output, new_state)
 

time: 71.7 us -> 70.9 us (0.989)
  local copies, waits for them, and re-layouts: 1.42 us -> 0 us
    unnamed x2 -> x0, local copies, waits for them, and re-layouts: 1.42 us -> none
    pallas_call x0 -> x1, Pallas kernels: none -> 0.83 us  [to_memory(): pl.pallas_call(write_out, out_shape=tuple((jax.ShapeDtypeStruct(a.shape,...]
where the time goes in v5:
time: 70.9 us; the launch traced here: 70.7 us
  Pallas kernels  70.1 us (99%)
    pallas_call x1, Pallas kernels, layer(): pl.pallas_call(functools.partial(layer_kernel, side, cap, experts, names)...  69.3 us

profile of v5, /device:TPU:513, one launch (start us, length us, event | category | flops | bytes accessed | tf_op | source)
XLA Modules:
  0.0 70.7 jit_solution(6661455803162423246)
XLA Ops:
  0.6 69.3 %layer.1 = (bf16[32,1024]{1,0:T(8,128)(2,1)S(1)}, f32[1024,64]{1,0:T(8,128)S(1)}) custom-call(s32[6,32]{1,0:T(8,128)} %bitcast.21, f32[6,32]{1,0:T(8,128)} %bitcast.22, f32[16,64]{1,0:T(8,128)} %refs_2_.1, f32[16,64]{1,0:T(8,128)} %refs_3_.1, f32[1,16]{1,0:T(1,128)} %bitcast.26, f32[2,16,16,64]{3,2,1,0:T(8,128)} %bitcast.18, f32[2,16,16,64]{3,2,1,0:T(8,128)} %refs_6_.1, ...), custom_call_target="tpu_custom_call" | custom-call | tf_op jit(solution)/shard_map/layer/pallas_call | solution.py:532
  69.9 0.8 %write_out.1 = (bf16[32,1024]{1,0:T(8,128)(2,1)}, f32[1024,64]{1,0:T(8,128)}) custom-call(bf16[32,1024]{1,0:T(8,128)(2,1)S(1)} %get-tuple-element.6.refs_0_, f32[1024,64]{1,0:T(8,128)S(1)} %get-tuple-element.7.refs_1_), custom_call_target="tpu_custom_call" | custom-call | tf_op jit(solution)/shard_map/write_out/pallas_call | solution.py:594

commit v6 on v5

--- a/solution.py
+++ b/solution.py
@@ -372,6 +372,12 @@
     shared_copy = go(to_partner(4 + 2 * side, sh_send, sh_recv))
     shared_own = dot(hidden, ds_v[:, pl.ds(pl.multiple_of(base, 128), half)]).astype(bf16)
 
+    mine = parts_of(iota((every, 1), 0))
+    theirs = parts_of(iota((1, every), 1))
+    swap = jnp.where(
+        (mine[0] == theirs[1]) & (mine[1] == theirs[0]) & (mine[2] == theirs[2]), 1.0, 0.0
+    ).astype(bf16)
+
     for h in range(2):
         first_ones = [1, -1] if h == 0 else [3, -3, 4]
         if not tree:
@@ -385,12 +391,6 @@
                 XS + h, cross_peer(d), x_send.at[h, place], x_recv.at[h, slot(-d)], place, slot(-d)
             )
         x_recv[h, 0] = x_send[h, 0]
-
-    mine = parts_of(iota((every, 1), 0))
-    theirs = parts_of(iota((1, every), 1))
-    swap = jnp.where(
-        (mine[0] == theirs[1]) & (mine[1] == theirs[0]) & (mine[2] == theirs[2]), 1.0, 0.0
-    ).astype(bf16)
 
     def hand_over(h, k):
         return to_partner(4 + h * side + k, x_recv.at[h, k], x_oth.at[h, k])

time: 70.9 us -> 70.9 us (level)
  no operation moved by 1% of the time
where the time goes in v6:
time: 70.9 us; the launch traced here: 70.8 us
  Pallas kernels  70.1 us (99%)
    pallas_call x1, Pallas kernels, layer(): pl.pallas_call(functools.partial(layer_kernel, side, cap, experts, names)...  69.3 us

profile of v6, /device:TPU:513, one launch (start us, length us, event | category | flops | bytes accessed | tf_op | source)
XLA Modules:
  0.0 70.8 jit_solution(9656957389524595915)
XLA Ops:
  0.6 69.3 %layer.1 = (bf16[32,1024]{1,0:T(8,128)(2,1)S(1)}, f32[1024,64]{1,0:T(8,128)S(1)}) custom-call(s32[6,32]{1,0:T(8,128)} %bitcast.21, f32[6,32]{1,0:T(8,128)} %bitcast.22, f32[16,64]{1,0:T(8,128)} %refs_2_.1, f32[16,64]{1,0:T(8,128)} %refs_3_.1, f32[1,16]{1,0:T(1,128)} %bitcast.26, f32[2,16,16,64]{3,2,1,0:T(8,128)} %bitcast.18, f32[2,16,16,64]{3,2,1,0:T(8,128)} %refs_6_.1, ...), custom_call_target="tpu_custom_call" | custom-call | tf_op jit(solution)/shard_map/layer/pallas_call | solution.py:532
  69.9 0.8 %write_out.1 = (bf16[32,1024]{1,0:T(8,128)(2,1)}, f32[1024,64]{1,0:T(8,128)}) custom-call(bf16[32,1024]{1,0:T(8,128)(2,1)S(1)} %get-tuple-element.6.refs_0_, f32[1024,64]{1,0:T(8,128)S(1)} %get-tuple-element.7.refs_1_), custom_call_target="tpu_custom_call" | custom-call | tf_op jit(solution)/shard_map/write_out/pallas_call | solution.py:594
